TPU v7x, 32 devices: a whole 2x2x4 slice. The times are simulated.
32 devices in a mesh: sp: 16 (over z, y, x), tp: 2 (over core).
Axes of the slice: x: 2, y: 2, z: 4, core: 2. Of those that a mesh axis runs over, the one named last changes fastest.
Arguments:
- mixer_in: bfloat16 [8192, 1024], P('sp', 'tp'), may hold values from -6 to 6
- residual: bfloat16 [8192, 2048], P(('sp', 'tp')), may hold values from -6 to 6
- decay_real: float32 [64, 64], P('tp'), may hold values from -2 to 0, as said below
- decay_imag: float32 [64, 64], P('tp'), may hold values from 1 to 200
- log_step: float32 [64], P('tp'), may hold values from -3.9 to -2.5
- in_real: float32 [64, 64, 16], P('tp'), may hold values from -1 to 1
- in_imag: float32 [64, 64, 16], P('tp'), may hold values from -1 to 1
- output_real: float32 [64, 16, 64], P('tp'), may hold values from -0.5 to 0.5
- output_imaginary: float32 [64, 16, 64], P('tp'), may hold values from -0.5 to 0.5
- skip: float32 [1024], P('tp'), may hold values from -4 to 4
- out_proj: bfloat16 [1024, 2048], P('tp'), may hold values from -0.1875 to 0.1875
- norm_gain: float32 [2048], replicated, may hold values from 0.1 to 1.9
- w_gate: bfloat16 [2048, 5632], P('sp', 'tp'), may hold values from -0.125 to 0.125
- w_up: bfloat16 [2048, 5632], P('sp', 'tp'), may hold values from -0.125 to 0.125
- w_down: bfloat16 [5632, 2048], P('tp', 'sp'), may hold values from -0.078125 to 0.078125
Outputs:
- output: bfloat16 [8192, 2048], P(('sp', 'tp'))
Inputs may be any that keep to these rules, and one draw needn't show every extreme that they name: `decay_real`: every entry is negative.
All inputs are finite; a program needn't handle non-finite values.
Results may differ from a plain program's by a relative error of at most 0.02.
Values may be sent and summed in bfloat16 or wider, within the bound.
A program may use at most 128 MiB of HBM per device.

v0:
```python
import functools

import jax
import jax.numpy as jnp
from jax import lax
from jax.experimental import pallas as pl
from jax.experimental.pallas import tpu as pltpu
from jax.sharding import Mesh
from jax.sharding import PartitionSpec as P

F32 = jnp.float32
BF16 = jnp.bfloat16
SP = ("h", "u", "m", "v")
PEERS = ("u", "v")
GATHER = 8
CHUNKS = 8
MESH = pl.DeviceIdType.MESH


def discrete(decay_real, decay_imag, log_step, in_real, in_imag):
    step_size = jnp.exp(log_step)[:, None]
    magnitude = jnp.exp(decay_real * step_size)
    angle = decay_imag * step_size
    power_re = magnitude * jnp.cos(angle)
    power_im = magnitude * jnp.sin(angle)
    denom = decay_real * decay_real + decay_imag * decay_imag
    ratio_re = ((power_re - 1.0) * decay_real + power_im * decay_imag) / denom
    ratio_im = (power_im * decay_real - (power_re - 1.0) * decay_imag) / denom
    drive_re = ratio_re[..., None] * in_real - ratio_im[..., None] * in_imag
    drive_im = ratio_re[..., None] * in_imag + ratio_im[..., None] * in_real
    return (power_re, power_im, drive_re, drive_im)


def cmul(ar, ai, br, bi):
    return ar * br - ai * bi, ar * bi + ai * br


def cpow(ar, ai, count):
    result = None
    while count:
        if count & 1:
            result = (ar, ai) if result is None else cmul(*result, ar, ai)
        count >>= 1
        if count:
            ar, ai = cmul(ar, ai, ar, ai)
    return result


def iota(shape, dim):
    return lax.broadcasted_iota(jnp.int32, shape, dim)


def tiled(block, copies, across, down):
    rows, columns = block.shape
    wide = (columns, columns * copies)
    pick = (iota(wide, 0) == lax.rem(iota(wide, 1), columns)).astype(BF16)
    full = jnp.dot(block, pick, preferred_element_type=F32)
    keep = lax.div(iota(full.shape, 0), down) == lax.div(iota(full.shape, 1), across)
    return jnp.where(keep, full, 0.0).astype(BF16)


def layer(sizes, fused, x_ref, b_ref, c_ref, a_ref, k_ref, wo_ref, res_ref, gain_ref, *rest):
    quarters, rest = rest[:3], rest[3:]
    if fused:
        out_ref, *rest = rest
        hidden, partners, peers, *rest = rest
    weights, (rows_ref, carried_ref), rest = rest[:3], rest[3:5], rest[5:]
    (work, read_in, read_out, ends, total, gathered, act, share, others,
     send_sem, recv_sem, local_sem) = rest
    blocks, rows, cb = x_ref.shape
    sb = a_ref.shape[2]
    depth = quarters[0].shape[2]
    width = wo_ref.shape[1]
    span = rows // CHUNKS
    nh, nm, tp = sizes["h"], sizes["m"], sizes["tp"]
    n = nh * 4 * nm
    h, u, m, v, core = (lax.axis_index(name) for name in (*SP, "tp"))
    index = lambda h, u, m, v: ((h * 2 + u) * nm + m) * 2 + v
    me = index(h, u, m, v)
    peer = lambda k: (1 - u if k & 2 else u, 1 - v if k & 1 else v)
    counter = iter(range(send_sem.shape[0]))

    def send(src, dst, device):
        slot = next(counter)
        copy = pltpu.make_async_remote_copy(
            src_ref=src, dst_ref=dst, send_sem=send_sem.at[slot], recv_sem=recv_sem.at[slot],
            device_id=device, device_id_type=MESH,
        )
        copy.start()
        return copy

    def place(ref, position):
        if depth % 128:
            return ref.at[position]
        return ref.at[:, pl.ds(pl.multiple_of(position * depth, depth), depth)]

    barrier = pltpu.get_barrier_semaphore()
    others_sp = []
    for k in range(1, n):
        to = lax.rem(me + k, n)
        there = (lax.div(to, 4 * nm), lax.rem(lax.div(to, 2 * nm), 2),
                 lax.rem(lax.div(to, 2), nm), lax.rem(to, 2), core)
        others_sp.append(there)
        pl.semaphore_signal(barrier, inc=1, device_id=there, device_id_type=MESH)
    for t in range(1, tp):
        pl.semaphore_signal(
            barrier, inc=1, device_id=(h, u, m, v, lax.rem(core + t, tp)), device_id_type=MESH
        )
    pl.semaphore_wait(barrier, n - 1 + tp - 1)

    sent = []
    first = {}
    over_h = {}
    over_m = {}

    def spread_h(w, k, src, position):
        for r in range(1, nh):
            pu, pv = peer(k)
            copy = send(src, place(weights[w], position), (lax.rem(h + r, nh), u, m, v, core))
            over_h[w, k, r] = copy

    def spread_m(w, k, r, src, position):
        for s in range(1, nm):
            over_m[w, k, r, s] = send(
                src, place(weights[w], position), (h, u, lax.rem(m + s, nm), v, core)
            )

    own = u * 2 + v
    for w in range(3):
        for k in (3, 1, 2):
            pu, pv = peer(k)
            first[w, k] = send(
                quarters[w].at[pu * 2 + pv], place(weights[w], me), (h, pu, m, pv, core)
            )
    locals_ = []
    for w in range(3):
        spread_h(w, 0, quarters[w].at[own], me)
        spread_m(w, 0, 0, quarters[w].at[own], me)
        copy = pltpu.make_async_copy(quarters[w].at[own], place(weights[w], me), local_sem.at[w])
        copy.start()
        locals_.append(copy)

    def scan(b, start, keep):
        work[...] = jnp.dot(x_ref[b], read_in[b], preferred_element_type=F32)
        br = jnp.broadcast_to(a_ref[b, 0:1, :], (CHUNKS, sb))
        bi = jnp.broadcast_to(a_ref[b, 1:2, :], (CHUNKS, sb))

        def step(i, state):
            at = pl.ds(pl.multiple_of(i * CHUNKS, CHUNKS), CHUNKS)
            nr, ni = cmul(br, bi, *state)
            nr, ni = nr + work[at, :sb], ni + work[at, sb:]
            if keep:
                work[at, :sb] = nr
                work[at, sb:] = ni
            return nr, ni

        return lax.fori_loop(0, span, step, start, unroll=8)

    @pl.loop(0, blocks)
    def _(b):
        states = b_ref.shape[3]
        for half in range(2):
            read_in[b, :, half * sb:(half + 1) * sb] = tiled(
                b_ref[b, half], GATHER, states, cb // GATHER
            )
            read_out[b, half * sb:(half + 1) * sb, :] = tiled(
                c_ref[b, half], GATHER, cb // GATHER, states
            )
        zero = jnp.zeros((CHUNKS, sb), F32)
        sr, si = scan(b, (zero, zero), False)
        ends[b, :, :sb] = sr
        ends[b, :, sb:] = si
        lr, li = cpow(a_ref[b, 0:1, :], a_ref[b, 1:2, :], span)
        er, ei = sr[0:1], si[0:1]
        for chunk in range(1, CHUNKS):
            er, ei = cmul(lr, li, er, ei)
            er, ei = er + sr[chunk:chunk + 1], ei + si[chunk:chunk + 1]
        total[b, :, :sb] = er
        total[b, :, sb:] = ei

    states_out = [send(total, gathered.at[me], there) for there in others_sp]
    gathered[me] = total[...]
    for copy in states_out:
        copy.wait_recv()

    @pl.loop(0, blocks)
    def _(b):
        lr, li = cpow(a_ref[b, 0:1, :], a_ref[b, 1:2, :], span)
        tr, ti = cpow(lr, li, CHUNKS)
        hr = jnp.zeros((1, sb), F32)
        hi = hr
        for device in range(n - 1):
            nr, ni = cmul(tr, ti, hr, hi)
            nr = nr + gathered[device, b, :, :sb]
            ni = ni + gathered[device, b, :, sb:]
            hr, hi = jnp.where(device < me, nr, hr), jnp.where(device < me, ni, hi)
        starts_r, starts_i = [hr], [hi]
        for chunk in range(CHUNKS - 1):
            nr, ni = cmul(lr, li, hr, hi)
            hr = nr + ends[b, chunk:chunk + 1, :sb]
            hi = ni + ends[b, chunk:chunk + 1, sb:]
            starts_r.append(hr)
            starts_i.append(hi)
        scan(b, (jnp.concatenate(starts_r, axis=0), jnp.concatenate(starts_i, axis=0)), True)
        mixed = jnp.dot(work[...].astype(BF16), read_out[b], preferred_element_type=F32)
        mixed = mixed + k_ref[b] * x_ref[b].astype(F32)
        mixed = jax.nn.gelu(mixed).astype(BF16)
        square = (rows, rows)
        source = lax.rem(iota(square, 0), span) * CHUNKS + lax.div(iota(square, 0), span)
        turn = (iota(square, 1) == source).astype(BF16)
        act[:, pl.ds(pl.multiple_of(b * cb, cb), cb)] = jnp.dot(
            turn, mixed, preferred_element_type=F32
        ).astype(BF16)

    keep_rows = rows // tp
    tile = min(512, width)
    mixed_copies = []
    for t in (*range(1, tp), 0):
        to = lax.rem(core + t, tp)

        @pl.loop(0, width // tile)
        def _(j):
            at = pl.ds(pl.multiple_of(j * tile, tile), tile)
            share[t, :, at] = jnp.dot(
                act[pl.ds(pl.multiple_of(to * keep_rows, keep_rows), keep_rows), :],
                wo_ref[:, at], preferred_element_type=F32,
            ).astype(BF16)

        if t:
            mixed_copies.append(send(share.at[t], others.at[t - 1], (h, u, m, v, to)))

    for w in range(3):
        for k in (1, 2, 3):
            first[w, k].wait_recv()
            pu, pv = peer(k)
            position = index(h, pu, m, pv)
            spread_h(w, k, place(weights[w], position), position)
            spread_m(w, k, 0, place(weights[w], position), position)

    for copy in mixed_copies:
        copy.wait_recv()
    line = min(32, keep_rows)

    @pl.loop(0, keep_rows // line)
    def _(i):
        at = pl.ds(pl.multiple_of(i * line, line), line)
        mixed = share[0, at, :].astype(F32)
        for t in range(1, tp):
            mixed = mixed + others[t - 1, at, :].astype(F32)
        carried = res_ref[at, :].astype(F32) + mixed.astype(BF16).astype(F32)
        scale = lax.rsqrt(jnp.mean(carried * carried, axis=-1, keepdims=True) + 1e-06)
        carried_ref[at, :] = carried
        rows_ref[0, 0, at, :] = (carried * scale * gain_ref[...]).astype(BF16)

    row_copies = {}
    for k in (3, 1, 2):
        pu, pv = peer(k)
        row_copies[k] = send(rows_ref.at[0, 0], rows_ref.at[0, k], (h, pu, m, pv, core))
    last = []
    for t in range(1, tp):
        last.append(send(rows_ref.at[0, 0], rows_ref.at[t, 0], (h, u, m, v, lax.rem(core + t, tp))))

    def pass_m(w, k):
        pu, pv = peer(k)
        for r in range(1, nh):
            over_h[w, k, r].wait_recv()
            position = index(lax.rem(h - r + nh, nh), pu, m, pv)
            spread_m(w, k, r, place(weights[w], position), position)

    for w in range(3):
        for k in range(4):
            pass_m(w, k)
        if w == 1:
            for k in (1, 2, 3):
                row_copies[k].wait_recv()
                for t in range(1, tp):
                    last.append(send(
                        rows_ref.at[0, k], rows_ref.at[t, k], (h, u, m, v, lax.rem(core + t, tp))
                    ))
    sent = [*first.values(), *over_h.values(), *over_m.values(), *states_out, *mixed_copies]
    row_sends = [*row_copies.values(), *last]
    for (w, *_), copy in over_m.items():
        if w < 2 or not fused:
            copy.wait_recv()
    for copy in last:
        copy.wait_recv()
    for copy in locals_:
        copy.wait()
    if fused:
        sent += back(
            sizes, send, peer, (h, u, m, v, core), weights, rows_ref, carried_ref, out_ref,
            hidden, partners, peers, row_sends, [c for (w, *_), c in over_m.items() if w == 2],
        )
    else:
        sent += row_sends
    for copy in sent:
        copy.wait_send()


def back(sizes, send, peer, here, weights, rows_ref, carried_ref, out_ref, hidden, partners,
         peers, row_sends, down_copies):
    tp = sizes["tp"]
    h, u, m, v, core = here
    _, _, keep_rows, width = rows_ref.shape
    across = (((1,), (1,)), ((), ()))

    @pl.loop(0, 4 * tp)
    def _(i):
        t, k = lax.div(i, 4), lax.rem(i, 4)
        block = rows_ref[t, k]
        gate = lax.dot_general(block, weights[0][...], across, preferred_element_type=F32)
        up = lax.dot_general(block, weights[1][...], across, preferred_element_type=F32)
        hidden[i] = (jax.nn.silu(gate) * up).astype(BF16)

    for copy in (*down_copies,):
        copy.wait_recv()
    for copy in row_sends:
        copy.wait_send()

    tile = min(512, width)
    line = min(32, keep_rows)
    sent = []
    peer_copies = []
    from_core = {}

    def reduce(k):
        for copy in from_core[k]:
            copy.wait_recv()

        @pl.loop(0, keep_rows // line)
        def _(i):
            at = pl.ds(pl.multiple_of(i * line, line), line)
            total = rows_ref[0, k, at, :].astype(F32)
            for t in range(1, tp):
                total = total + partners[k, t - 1, at, :].astype(F32)
            rows_ref[0, k, at, :] = total.astype(BF16)

        if k:
            pu, pv = peer(k)
            peer_copies.append(send(rows_ref.at[0, k], peers.at[k - 1], (h, pu, m, pv, core)))

    order = (3, 1, 2, 0)
    for step, k in enumerate(order):
        from_core[k] = []
        for t in (*range(1, tp), 0):
            @pl.loop(0, width // tile)
            def _(j):
                at = pl.ds(pl.multiple_of(j * tile, tile), tile)
                rows_ref[t, k, :, at] = jnp.dot(
                    hidden[t * 4 + k], weights[2][:, at], preferred_element_type=F32
                ).astype(BF16)

            if t:
                from_core[k].append(send(
                    rows_ref.at[t, k], partners.at[k, t - 1],
                    (h, u, m, v, lax.rem(core + tp - t, tp)),
                ))
        reduce(k)
        sent += from_core[k]
    for copy in peer_copies:
        copy.wait_recv()

    @pl.loop(0, keep_rows // line)
    def _(i):
        at = pl.ds(pl.multiple_of(i * line, line), line)
        total = rows_ref[0, 0, at, :].astype(F32)
        for k in range(1, 4):
            total = total + peers[k - 1, at, :].astype(F32)
        total = total.astype(BF16).astype(F32)
        out_ref[at, :] = (carried_ref[at, :] + 0.5 * total).astype(BF16)

    return sent + peer_copies


def shift(value, axis, count, by):
    return lax.ppermute(value, axis, [(i, (i + by) % count) for i in range(count)])


def flip(value, axes, count, k):
    return lax.ppermute(value, axes, [(i, i ^ k) for i in range(count)])


def on_device(sizes, mixer_in, residual, decay_real, decay_imag, log_step, in_real, in_imag,
              output_real, output_imaginary, skip, out_proj, norm_gain, w_gate, w_up, w_down):
    tp, nh, nm = sizes["tp"], sizes["h"], sizes["m"]
    n = nh * 4 * nm
    rows, channels = mixer_in.shape
    keep_rows, width = residual.shape
    depth, hidden_units = w_gate.shape
    part = hidden_units // 4
    groups, states = decay_real.shape
    blocks = groups // GATHER
    cb, sb = channels // blocks, GATHER * states
    power_re, power_im, bar_re, bar_im = discrete(
        decay_real, decay_imag, log_step, in_real, in_imag
    )
    rows_first = lambda t: jnp.transpose(t, (0, 2, 1)).reshape(blocks, -1, t.shape[1])
    read_in = jnp.stack([rows_first(bar_re), rows_first(bar_im)], axis=1).astype(BF16)
    read_out = jnp.stack(
        [rows_first(output_real), -rows_first(output_imaginary)], axis=1
    ).astype(BF16)
    power = jnp.stack([power_re.reshape(blocks, sb), power_im.reshape(blocks, sb)], axis=1)
    x = mixer_in.reshape(CHUNKS, rows // CHUNKS, blocks, cb).transpose(2, 1, 0, 3)
    x = x.reshape(blocks, rows, cb)
    copies = 3 * (3 + 4 * (nh - 1) + 4 * nh * (nm - 1)) + (n - 1) + (tp - 1) + 3 + 4 * (tp - 1)
    laid = (part, n * depth) if depth % 128 == 0 else (n, part, depth)
    vmem = pl.BlockSpec(memory_space=pltpu.VMEM)
    between = [(laid, BF16)] * 3 + [
        ((tp, 4, keep_rows, width), BF16), ((keep_rows, width), F32),
    ]
    fused = depth % 128 == 0
    if fused:
        copies += 4 * (tp - 1) + 3
        out_shape = [jax.ShapeDtypeStruct((keep_rows, width), BF16)]
        extra = [
            pltpu.VMEM((4 * tp, keep_rows, part), BF16),
            pltpu.VMEM((4, tp - 1, keep_rows, width), BF16),
            pltpu.VMEM((3, keep_rows, width), BF16),
            *(pltpu.VMEM(*item) for item in between),
        ]
    else:
        out_shape = [jax.ShapeDtypeStruct(*item) for item in between]
        extra = []
    results = pl.pallas_call(
        functools.partial(layer, sizes, fused),
        in_specs=[vmem] * 11,
        out_specs=[vmem] * len(out_shape),
        out_shape=out_shape,
        scratch_shapes=[
            *extra,
            pltpu.VMEM((rows, 2 * sb), F32),
            pltpu.VMEM((blocks, cb, 2 * sb), BF16),
            pltpu.VMEM((blocks, 2 * sb, cb), BF16),
            pltpu.VMEM((blocks, CHUNKS, 2 * sb), F32),
            pltpu.VMEM((blocks, 1, 2 * sb), F32),
            pltpu.VMEM((n, blocks, 1, 2 * sb), F32),
            pltpu.VMEM((rows, channels), BF16),
            pltpu.VMEM((tp, keep_rows, width), BF16),
            pltpu.VMEM((tp - 1, keep_rows, width), BF16),
            pltpu.SemaphoreType.DMA((copies,)),
            pltpu.SemaphoreType.DMA((copies,)),
            pltpu.SemaphoreType.DMA((3,)),
        ],
        compiler_params=pltpu.CompilerParams(
            collective_id=0, has_side_effects=True, vmem_limit_bytes=62 * 2**20
        ),
        name="layer",
    )(x, read_in, read_out, power, skip.reshape(blocks, 1, cb), out_proj, residual,
      norm_gain.reshape(1, width), w_gate.T.reshape(4, part, depth),
      w_up.T.reshape(4, part, depth), w_down.reshape(4, part, depth))
    if fused:
        return results[0]
    full_gate, full_up, full_down, rows_all, carried = results
    if len(laid) == 3:
        full_gate, full_up, full_down = (
            t.transpose(1, 0, 2).reshape(part, width) for t in (full_gate, full_up, full_down)
        )

    flat = rows_all.reshape(-1, width)
    across = (((1,), (1,)), ((), ()))
    gate = lax.dot_general(flat, full_gate, across, preferred_element_type=F32)
    up = lax.dot_general(flat, full_up, across, preferred_element_type=F32)
    hidden = (jax.nn.silu(gate) * up).astype(BF16)
    down = jnp.dot(hidden, full_down, preferred_element_type=F32).astype(BF16)
    down = down.reshape(rows_all.shape)
    summed = down[0].astype(F32)
    for t in range(1, tp):
        summed = summed + shift(down[t], "tp", tp, -t).astype(F32)
    summed = summed.astype(BF16)
    total = summed[0].astype(F32)
    for k in range(1, 4):
        total = total + flip(summed[k], PEERS, 4, k).astype(F32)
    total = total.astype(BF16)
    return (carried + 0.5 * total.astype(F32)).astype(BF16)


def solution(mesh):
    sp, tp = mesh.shape["sp"], mesh.shape["tp"]
    sizes = {"h": sp // 8, "u": 2, "m": 2, "v": 2, "tp": tp}
    cut = Mesh(mesh.devices.reshape(tuple(sizes.values())), tuple(sizes))
    return jax.shard_map(
        functools.partial(on_device, sizes),
        mesh=cut,
        in_specs=(
            P(SP, "tp"),
            P((*SP, "tp"), None),
            P("tp", None),
            P("tp", None),
            P("tp"),
            P("tp", None, None),
            P("tp", None, None),
            P("tp", None, None),
            P("tp", None, None),
            P("tp"),
            P("tp", None),
            P(),
            P(SP, "tp"),
            P(SP, "tp"),
            P("tp", SP),
        ),
        out_specs=P((*SP, "tp"), None),
        check_vma=False,
    )
```

profile of v0, /device:TPU:0, one launch (start us, length us, event | category | flops | bytes accessed | tf_op | source)
XLA Modules:
  0.0 228.3 jit_solution(12036325246399897482)
XLA Ops:
  0.0 0.7 exp.6
  0.7 0.9 cosine_multiply_fusion
  1.6 0.1 stack_reshape.21
  1.6 0.1 stack_reshape.22
  1.7 0.6 pad_maximum_fusion.2.a_ref
  2.3 1.0 convert_bitcast_fusion
  3.3 1.0 fusion
  4.3 1.1 subtract_convert_fusion
  5.4 0.0 copy-start.2
  5.4 0.8 pad_maximum_fusion.1.b_ref
  6.2 0.3 copy.41
  6.5 0.3 copy.40
  6.8 0.0 copy-start
  6.8 1.2 pad_maximum_fusion.c_ref
  8.0 0.0 copy-done.2
  8.0 0.0 copy-start.1
  8.0 0.1 reshape.37
  8.1 1.1 copy.45
  9.2 0.0 copy-done
  9.2 1.2 copy.38
  10.4 0.0 copy-done.1
  10.4 1.1 copy.39
  11.5 214.5 %layer.1 = bf16[256,2048]{1,0:T(8,128)(2,1)} custom-call(bf16[4,512,128]{2,1,0:T(8,128)(2,1)} %bitcast.28, bf16[4,2,128,64]{3,2,1,0:T(8,128)(2,1)} %pad_maximum_fusion.1.b_ref, bf16[4,2,512,16]{3,2,1,0:T(8,128)(2,1)} %pad_maximum_fusion.c_ref, f32[4,2,512]{2,1,0:T(2,128)} %pad_maximum_fusion.2.a_ref, f32[4,1,128]{2,1,0:T(1,128)} %bitcast.35, ...), custom_call_target="tpu_custom_call" | custom-call | tf_op jit(solution)/shard_map/layer/pallas_call | solution.py:424
  226.0 2.3 %copy.47 = bf16[256,2048]{1,0:T(8,128)(2,1)} copy(bf16[256,2048]{1,0:T(8,128)(2,1)} %layer.1) | data formatting | bytes 2097152
Async XLA Ops:
  5.4 2.6 %copy-start.2 = (bf16[512,512]{1,0:T(8,128)(2,1)S(1)}, bf16[512,512]{1,0:T(8,128)(2,1)}, u32[]{:S(2)}) copy-start(bf16[512,512]{1,0:T(8,128)(2,1)} %param.15) | copy-start | bytes 1572868
  6.8 2.5 %copy-start = (bf16[128,2816]{1,0:T(8,128)(2,1)S(1)}, bf16[128,2816]{1,0:T(8,128)(2,1)}, u32[]{:S(2)}) copy-start(bf16[128,2816]{1,0:T(8,128)(2,1)} %param.27) | copy-start | bytes 2162692
  8.0 2.5 %copy-start.1 = (bf16[128,2816]{1,0:T(8,128)(2,1)S(1)}, bf16[128,2816]{1,0:T(8,128)(2,1)}, u32[]{:S(2)}) copy-start(bf16[128,2816]{1,0:T(8,128)(2,1)} %param.28) | copy-start | bytes 2162692
where the time goes:
time: 229 us; the launch traced here: 228 us
  Pallas kernels  214 us (93%)
  local copies, waits for them, and re-layouts  7.27 us (3%)
  other arithmetic  6.54 us (3%)
    pallas_call x1, Pallas kernels, on_device(): pl.pallas_call(functools.partial(layer, sizes, fused), in_specs=[vmem] *...  214 us

commit v1 on v0

--- a/solution.py
+++ b/solution.py
@@ -372,6 +372,469 @@
     return sent + peer_copies
 
 
+def streamed(sizes, scopes, x_ref, b_ref, c_ref, a_ref, k_ref, wo_ref, res_ref, gain_ref, gate_ref,
+             up_ref, down_ref, out_ref, *rest):
+    quarters, weights, rest = (gate_ref, up_ref, down_ref), rest[:3], rest[3:]
+    (extra, rows_ref, carried_ref, gates, hidden, partners, firsts, seconds, work, read_in,
+     read_out, ends, total, gathered, act, share, others, send_sem, recv_sem, local_sem) = rest
+    blocks, rows, cb = x_ref.shape
+    sb = a_ref.shape[2]
+    depth = gate_ref.shape[2]
+    width = wo_ref.shape[1]
+    keep_rows = rows // 2
+    span = rows // CHUNKS
+    nh, nm = sizes["h"], sizes["m"]
+    n = nh * 4 * nm
+    h, u, m, v, core = (lax.axis_index(name) for name in (*SP, "tp"))
+    oh, ou, om, ov = 1 - h, 1 - u, 1 - m, 1 - v
+    index = lambda h, u, m, v: ((h * 2 + u) * nm + m) * 2 + v
+    me = index(h, u, m, v)
+    inner = u != h
+    to_x, to_z, to_y = (h, u, m, ov, core), (h, ou, m, v, core), (h, u, om, v, core)
+    to_c, to_b, to_t = (oh, u, m, v, core), (oh, ou, m, v, core), (h, u, m, v, 1 - core)
+    plane = [(a, b, c) for a in (h, oh) for b in (u, ou) for c in (v, ov)]
+    across = (((1,), (1,)), ((), ()))
+    slots, everywhere, inside, moves = {}, [], [], []
+    counter = iter(range(send_sem.shape[0]))
+
+    def slot(name):
+        return slots.setdefault(name, len(slots))
+
+    def describe(src, dst, device, name, number):
+        return pltpu.make_async_remote_copy(
+            src_ref=src, dst_ref=dst, send_sem=send_sem.at[number],
+            recv_sem=recv_sem.at[slot(name)], device_id=device, device_id_type=MESH,
+        )
+
+    def send(src, dst, device, name, kept=everywhere):
+        number = next(counter)
+        copy = describe(src, dst, device, name, number)
+        copy.start()
+        kept.append((name, number) if kept is inside else copy)
+
+    def arrive(dst, device, name):
+        describe(dst, dst, device, name, 0).wait_recv()
+
+    def place(w, position):
+        return weights[w].at[:, pl.ds(pl.multiple_of(position * depth, depth), depth)]
+
+    def spot(w, j, row=m):
+        a, b, c = plane[j]
+        return place(w, index(a, b, row, c))
+
+    def mine(w, b, c):
+        return quarters[w].at[b * 2 + c]
+
+    def own(w):
+        return mine(w, u, v)
+
+    def send_x(w, s):
+        if s:
+            send(mine(w, ou, ov), extra.at[w], to_x, ("xo", w))
+        else:
+            send(mine(w, u, ov), spot(w, 0), to_x, ("xu", w))
+
+    def send_z(w, s):
+        send(extra.at[w] if s else mine(w, ou, v), spot(w, s), to_z, ("z", w, s))
+
+    def send_c(w, s):
+        send(spot(w, 1) if s else own(w), spot(w, s), to_c, ("cs", w, s))
+
+    def send_b(w, s):
+        send(extra.at[w] if s else mine(w, ou, v), spot(w, s), to_b, ("co", w, s), inside)
+
+    def relay(w, s):
+        send(spot(w, 2 + s), spot(w, 2 + s), to_c, ("co", w, s), inside)
+
+    def send_y(w, j):
+        send(own(w) if j == 0 else spot(w, j), spot(w, j), to_y, ("y", w, j))
+
+    def wait_x(w, s):
+        if s:
+            arrive(extra.at[w], to_x, ("xo", w))
+        else:
+            arrive(spot(w, 1), to_x, ("xu", w))
+
+    def wait_z(w, s):
+        arrive(spot(w, 2 + s), to_z, ("z", w, s))
+
+    def wait_cs(w, s):
+        arrive(spot(w, 4 + s), to_c, ("cs", w, s))
+
+    def wait_co(w, s):
+        arrive(spot(w, 6 + s), to_c, ("co", w, s))
+
+    def wait_y(w, j):
+        arrive(spot(w, j, om), to_y, ("y", w, j))
+
+    barrier = pltpu.get_barrier_semaphore()
+    others_sp = []
+    for k in range(1, n):
+        to = lax.rem(me + k, n)
+        there = (lax.div(to, 4 * nm), lax.rem(lax.div(to, 2 * nm), 2),
+                 lax.rem(lax.div(to, 2), nm), lax.rem(to, 2), core)
+        others_sp.append(there)
+        pl.semaphore_signal(barrier, inc=1, device_id=there, device_id_type=MESH)
+    pl.semaphore_signal(barrier, inc=1, device_id=to_t, device_id_type=MESH)
+    with jax.named_scope("A_barrier"):
+        pl.semaphore_wait(barrier, n)
+
+    send_x(0, 0)
+    send_z(0, 0)
+    send_y(0, 0)
+
+    @pl.when(inner)
+    def _():
+        send_b(0, 0)
+
+    local = []
+    for w in range(3):
+        copy = pltpu.make_async_copy(own(w), spot(w, 0), local_sem.at[w])
+        copy.start()
+        local.append(copy)
+
+    def scan(b, start, keep):
+        work[...] = jnp.dot(x_ref[b], read_in[b], preferred_element_type=F32)
+        br = jnp.broadcast_to(a_ref[b, 0:1, :], (CHUNKS, sb))
+        bi = jnp.broadcast_to(a_ref[b, 1:2, :], (CHUNKS, sb))
+
+        def step(i, state):
+            at = pl.ds(pl.multiple_of(i * CHUNKS, CHUNKS), CHUNKS)
+            nr, ni = cmul(br, bi, *state)
+            nr, ni = nr + work[at, :sb], ni + work[at, sb:]
+            if keep:
+                work[at, :sb] = nr
+                work[at, sb:] = ni
+            return nr, ni
+
+        return lax.fori_loop(0, span, step, start, unroll=8)
+
+    with jax.named_scope("B_scan1"):
+        @pl.loop(0, blocks)
+        def _(b):
+            states = b_ref.shape[3]
+            for half in range(2):
+                read_in[b, :, half * sb:(half + 1) * sb] = tiled(
+                    b_ref[b, half], GATHER, states, cb // GATHER
+                )
+                read_out[b, half * sb:(half + 1) * sb, :] = tiled(
+                    c_ref[b, half], GATHER, cb // GATHER, states
+                )
+            zero = jnp.zeros((CHUNKS, sb), F32)
+            sr, si = scan(b, (zero, zero), False)
+            ends[b, :, :sb] = sr
+            ends[b, :, sb:] = si
+            lr, li = cpow(a_ref[b, 0:1, :], a_ref[b, 1:2, :], span)
+            er, ei = sr[0:1], si[0:1]
+            for chunk in range(1, CHUNKS):
+                er, ei = cmul(lr, li, er, ei)
+                er, ei = er + sr[chunk:chunk + 1], ei + si[chunk:chunk + 1]
+            total[b, :, :sb] = er
+            total[b, :, sb:] = ei
+
+    for k, there in enumerate(others_sp):
+        send(total, gathered.at[me], there, ("s", k))
+    gathered[me] = total[...]
+
+    send_x(0, 1)
+    send_c(0, 0)
+    for w in (1, 2):
+        for s in range(2):
+            send_x(w, s)
+    with jax.named_scope("C_x0"):
+        wait_x(0, 0)
+    send_c(0, 1)
+    send_y(0, 1)
+    with jax.named_scope("C_states"):
+        for k in range(n - 1):
+            arrive(gathered.at[lax.rem(me + n - 1 - k, n)], others_sp[k], ("s", k))
+
+    square = (rows, rows)
+    source = lax.rem(iota(square, 0), span) * CHUNKS + lax.div(iota(square, 0), span)
+
+    with jax.named_scope("D_scan2"):
+        @pl.loop(0, blocks)
+        def _(b):
+            lr, li = cpow(a_ref[b, 0:1, :], a_ref[b, 1:2, :], span)
+            tr, ti = cpow(lr, li, CHUNKS)
+            hr = jnp.zeros((1, sb), F32)
+            hi = hr
+            for device in range(n - 1):
+                nr, ni = cmul(tr, ti, hr, hi)
+                nr = nr + gathered[device, b, :, :sb]
+                ni = ni + gathered[device, b, :, sb:]
+                hr, hi = jnp.where(device < me, nr, hr), jnp.where(device < me, ni, hi)
+            starts_r, starts_i = [hr], [hi]
+            for chunk in range(CHUNKS - 1):
+                nr, ni = cmul(lr, li, hr, hi)
+                hr = nr + ends[b, chunk:chunk + 1, :sb]
+                hi = ni + ends[b, chunk:chunk + 1, sb:]
+                starts_r.append(hr)
+                starts_i.append(hi)
+            scan(b, (jnp.concatenate(starts_r, axis=0), jnp.concatenate(starts_i, axis=0)), True)
+            mixed = jnp.dot(work[...].astype(BF16), read_out[b], preferred_element_type=F32)
+            mixed = mixed + k_ref[b] * x_ref[b].astype(F32)
+            mixed = jax.nn.gelu(mixed).astype(BF16)
+            turn = (iota(square, 1) == source).astype(BF16)
+            act[:, pl.ds(pl.multiple_of(b * cb, cb), cb)] = jnp.dot(
+                turn, mixed, preferred_element_type=F32
+            ).astype(BF16)
+
+    with jax.named_scope("D_x1"):
+        wait_x(0, 1)
+    send_z(0, 1)
+
+    @pl.when(inner)
+    def _():
+        send_b(0, 1)
+
+    tile = min(512, width)
+    with jax.named_scope("E_outproj"):
+        for t in (1, 0):
+            to = core if t == 0 else 1 - core
+
+            @pl.loop(0, width // tile)
+            def _(j):
+                at = pl.ds(pl.multiple_of(j * tile, tile), tile)
+                share[t, :, at] = jnp.dot(
+                    act[pl.ds(pl.multiple_of(to * keep_rows, keep_rows), keep_rows), :],
+                    wo_ref[:, at], preferred_element_type=F32,
+                ).astype(BF16)
+
+            if t:
+                send(share.at[1], others, to_t, ("mix",))
+
+    with jax.named_scope("G_mix"):
+        arrive(others, to_t, ("mix",))
+    line = min(32, keep_rows)
+    with jax.named_scope("H_norm"):
+        @pl.loop(0, keep_rows // line)
+        def _(i):
+            at = pl.ds(pl.multiple_of(i * line, line), line)
+            mixed = share[0, at, :].astype(F32) + others[at, :].astype(F32)
+            carried = res_ref[at, :].astype(F32) + mixed.astype(BF16).astype(F32)
+            scale = lax.rsqrt(jnp.mean(carried * carried, axis=-1, keepdims=True) + 1e-06)
+            carried_ref[at, :] = carried
+            rows_ref[0, 0, at, :] = (carried * scale * gain_ref[...]).astype(BF16)
+
+    send(rows_ref.at[0, 0], rows_ref.at[0, 1], to_x, ("r", 1), moves)
+    send(rows_ref.at[0, 0], rows_ref.at[0, 2], to_z, ("r", 2), moves)
+    send(rows_ref.at[0, 0], rows_ref.at[1, 0], to_t, ("t", 0), moves)
+
+    def share_core(k):
+        send(rows_ref.at[0, k], rows_ref.at[1, k], to_t, ("t", k), moves)
+
+    def wait_core(k):
+        arrive(rows_ref.at[1, k], to_t, ("t", k))
+
+    def own_blocks(w):
+        send_z(w, 0)
+        send_c(w, 0)
+        send_y(w, 0)
+
+        @pl.when(inner)
+        def _():
+            send_b(w, 0)
+
+        wait_x(w, 0)
+        send_c(w, 1)
+        send_y(w, 1)
+        wait_x(w, 1)
+        send_z(w, 1)
+
+        @pl.when(inner)
+        def _():
+            send_b(w, 1)
+
+    def pass_z(w):
+        for s in range(2):
+            with jax.named_scope(f"z{w}{s}"):
+                wait_z(w, s)
+
+            @pl.when(inner)
+            def _():
+                relay(w, s)
+
+            send_y(w, 2 + s)
+
+    def pass_c(w):
+        for s in range(2):
+            with jax.named_scope(f"cs{w}{s}"):
+                wait_cs(w, s)
+            send_y(w, 4 + s)
+
+    def pass_o(w):
+        for s in range(2):
+            with jax.named_scope(f"co{w}{s}"):
+                wait_co(w, s)
+            send_y(w, 6 + s)
+
+    def gate_part(t, k):
+        with jax.named_scope(f"gate{t}{k}"):
+            gates[4 * t + k] = lax.dot_general(
+                rows_ref[t, k], weights[0][...], across, preferred_element_type=F32
+            )
+
+    def up_part(t, k):
+        with jax.named_scope(f"up{t}{k}"):
+            up = lax.dot_general(
+                rows_ref[t, k], weights[1][...], across, preferred_element_type=F32
+            )
+            hidden[pl.ds((4 * t + k) * keep_rows, keep_rows), :] = (
+                jax.nn.silu(gates[4 * t + k]) * up
+            ).astype(BF16)
+
+    half = keep_rows // 2
+    with jax.named_scope("own1"):
+        own_blocks(1)
+    pass_z(0)
+    pass_c(0)
+    pass_o(0)
+    with jax.named_scope("r1"):
+        arrive(rows_ref.at[0, 1], to_x, ("r", 1))
+    send(rows_ref.at[0, 1, pl.ds(0, half)], rows_ref.at[0, 3, pl.ds(0, half)], to_z,
+         ("r", 3, 0), moves)
+    share_core(1)
+    with jax.named_scope("r2"):
+        arrive(rows_ref.at[0, 2], to_z, ("r", 2))
+    send(rows_ref.at[0, 2, pl.ds(half, half)], rows_ref.at[0, 3, pl.ds(half, half)], to_x,
+         ("r", 3, 1), moves)
+    share_core(2)
+    for copy in local:
+        copy.wait()
+    with jax.named_scope("y0"):
+        for j in range(8):
+            wait_y(0, j)
+    wait_core(0)
+    gate_part(0, 0)
+    gate_part(1, 0)
+    pass_z(1)
+    with jax.named_scope("own2"):
+        own_blocks(2)
+    gate_part(0, 1)
+    wait_core(1)
+    gate_part(1, 1)
+    pass_c(1)
+    gate_part(0, 2)
+    wait_core(2)
+    gate_part(1, 2)
+    pass_o(1)
+    with jax.named_scope("r3"):
+        arrive(rows_ref.at[0, 3, pl.ds(0, half)], to_z, ("r", 3, 0))
+        arrive(rows_ref.at[0, 3, pl.ds(half, half)], to_x, ("r", 3, 1))
+    share_core(3)
+    gate_part(0, 3)
+    pass_z(2)
+    with jax.named_scope("t3"):
+        wait_core(3)
+    gate_part(1, 3)
+    with jax.named_scope("y1"):
+        for j in range(8):
+            wait_y(1, j)
+    for t, k in ((0, 0), (1, 0), (0, 1)):
+        up_part(t, k)
+    pass_c(2)
+    for t, k in ((1, 1), (0, 2), (1, 2)):
+        up_part(t, k)
+    pass_o(2)
+    for t, k in ((0, 3), (1, 3)):
+        up_part(t, k)
+    with jax.named_scope("moves"):
+        for copy in moves:
+            copy.wait_send()
+
+    across_u = width // 8
+    chunks = [(a, b, c) for a in (h, oh) for c in (m, om) for b in range(2)]
+
+    def columns(j):
+        a, b, c = chunks[j]
+        return pl.ds(pl.multiple_of(index(a, b, c, 0) * depth, across_u), across_u)
+
+    def down(j):
+        at = columns(j)
+        for t in (1, 0):
+            result = jnp.dot(
+                hidden[4 * t * keep_rows:4 * (t + 1) * keep_rows, :], weights[2][:, at],
+                preferred_element_type=F32,
+            ).astype(BF16)
+            for k in range(4):
+                rows_ref[t, k, :, at] = result[k * keep_rows:(k + 1) * keep_rows]
+            if t:
+                send(rows_ref.at[1, :, :, at], partners.at[j], to_t, ("p", j))
+
+    def add(target, j, other):
+        at = columns(j)
+
+        @pl.loop(0, keep_rows // line)
+        def _(i):
+            lines = pl.ds(pl.multiple_of(i * line, line), line)
+            rows_ref[0, target, lines, at] = (
+                rows_ref[0, target, lines, at].astype(F32) + other[lines, :].astype(F32)
+            ).astype(BF16)
+
+    def pair(j):
+        at = columns(j)
+        near, far = (1, 2) if j % 2 == 0 else (2, 1)
+        device = to_x if j % 2 == 0 else to_z
+        arrive(partners.at[j], to_t, ("p", j))
+        for place_in, k in enumerate((3, near)):
+            add(k, j, partners.at[j, k])
+            send(rows_ref.at[0, k, :, at], firsts.at[j, place_in], device, ("f", j, place_in))
+        add(far, j, partners.at[j, far])
+        add(0, j, partners.at[j, 0])
+
+    def combine(j):
+        at = columns(j)
+        far = 2 if j % 2 == 0 else 1
+        device, other = (to_x, to_z) if j % 2 == 0 else (to_z, to_x)
+        arrive(firsts.at[j, 0], device, ("f", j, 0))
+        add(far, j, firsts.at[j, 0])
+        send(rows_ref.at[0, far, :, at], seconds.at[j], other, ("g", j))
+        arrive(firsts.at[j, 1], device, ("f", j, 1))
+        add(0, j, firsts.at[j, 1])
+
+    def finish(j):
+        at = columns(j)
+        arrive(seconds.at[j], to_z if j % 2 == 0 else to_x, ("g", j))
+
+        @pl.loop(0, keep_rows // line)
+        def _(i):
+            lines = pl.ds(pl.multiple_of(i * line, line), line)
+            summed = rows_ref[0, 0, lines, at].astype(F32) + seconds[j, lines, :].astype(F32)
+            summed = summed.astype(BF16).astype(F32)
+            out_ref[lines, at] = (carried_ref[lines, at] + 0.5 * summed).astype(BF16)
+
+    lag = (1, 3, 5)
+    for step in range(8 + lag[2]):
+        if step < 8:
+            if step == 2:
+                with jax.named_scope("y2a"):
+                    for j in range(4):
+                        wait_y(2, j)
+            if step == 6:
+                with jax.named_scope("y2b"):
+                    for j in range(4, 8):
+                        wait_y(2, j)
+            with jax.named_scope(f"down{step}"):
+                down(step)
+        if 0 <= step - lag[0] < 8:
+            with jax.named_scope(f"pair{step - lag[0]}"):
+                pair(step - lag[0])
+        if 0 <= step - lag[1] < 8:
+            with jax.named_scope(f"comb{step - lag[1]}"):
+                combine(step - lag[1])
+        if 0 <= step - lag[2] < 8:
+            with jax.named_scope(f"fin{step - lag[2]}"):
+                finish(step - lag[2])
+    for copy in everywhere:
+        copy.wait_send()
+
+    @pl.when(inner)
+    def _():
+        for name, number in inside:
+            describe(extra.at[0], extra.at[0], to_c, name, number).wait_send()
+
+
 def shift(value, axis, count, by):
     return lax.ppermute(value, axis, [(i, (i + by) % count) for i in range(count)])
 
@@ -402,9 +865,47 @@
     power = jnp.stack([power_re.reshape(blocks, sb), power_im.reshape(blocks, sb)], axis=1)
     x = mixer_in.reshape(CHUNKS, rows // CHUNKS, blocks, cb).transpose(2, 1, 0, 3)
     x = x.reshape(blocks, rows, cb)
+    vmem = pl.BlockSpec(memory_space=pltpu.VMEM)
+    operands = (x, read_in, read_out, power, skip.reshape(blocks, 1, cb), out_proj, residual,
+                norm_gain.reshape(1, width), w_gate.T.reshape(4, part, depth),
+                w_up.T.reshape(4, part, depth), w_down.reshape(4, part, depth))
+    if depth % 128 == 0 and (tp, nh, nm) == (2, 2, 2):
+        cut = width // 8
+        return pl.pallas_call(
+            functools.partial(streamed, sizes, None),
+            in_specs=[vmem] * 11,
+            out_specs=vmem,
+            out_shape=jax.ShapeDtypeStruct((keep_rows, width), BF16),
+            scratch_shapes=[
+                *[pltpu.VMEM((part, n * depth), BF16)] * 3,
+                pltpu.VMEM((3, part, depth), BF16),
+                pltpu.VMEM((2, 4, keep_rows, width), BF16),
+                pltpu.VMEM((keep_rows, width), F32),
+                pltpu.VMEM((8, keep_rows, part), F32),
+                pltpu.VMEM((8 * keep_rows, part), BF16),
+                pltpu.VMEM((8, 4, keep_rows, cut), BF16),
+                pltpu.VMEM((8, 2, keep_rows, cut), BF16),
+                pltpu.VMEM((8, keep_rows, cut), BF16),
+                pltpu.VMEM((rows, 2 * sb), F32),
+                pltpu.VMEM((blocks, cb, 2 * sb), BF16),
+                pltpu.VMEM((blocks, 2 * sb, cb), BF16),
+                pltpu.VMEM((blocks, CHUNKS, 2 * sb), F32),
+                pltpu.VMEM((blocks, 1, 2 * sb), F32),
+                pltpu.VMEM((n, blocks, 1, 2 * sb), F32),
+                pltpu.VMEM((rows, channels), BF16),
+                pltpu.VMEM((2, keep_rows, width), BF16),
+                pltpu.VMEM((keep_rows, width), BF16),
+                pltpu.SemaphoreType.DMA((160,)),
+                pltpu.SemaphoreType.DMA((160,)),
+                pltpu.SemaphoreType.DMA((3,)),
+            ],
+            compiler_params=pltpu.CompilerParams(
+                collective_id=0, has_side_effects=True, vmem_limit_bytes=62 * 2**20
+            ),
+            name="streamed",
+        )(*operands)
     copies = 3 * (3 + 4 * (nh - 1) + 4 * nh * (nm - 1)) + (n - 1) + (tp - 1) + 3 + 4 * (tp - 1)
     laid = (part, n * depth) if depth % 128 == 0 else (n, part, depth)
-    vmem = pl.BlockSpec(memory_space=pltpu.VMEM)
     between = [(laid, BF16)] * 3 + [
         ((tp, 4, keep_rows, width), BF16), ((keep_rows, width), F32),
     ]
@@ -445,9 +946,7 @@
             collective_id=0, has_side_effects=True, vmem_limit_bytes=62 * 2**20
         ),
         name="layer",
-    )(x, read_in, read_out, power, skip.reshape(blocks, 1, cb), out_proj, residual,
-      norm_gain.reshape(1, width), w_gate.T.reshape(4, part, depth),
-      w_up.T.reshape(4, part, depth), w_down.reshape(4, part, depth))
+    )(*operands)
     if fused:
         return results[0]
     full_gate, full_up, full_down, rows_all, carried = results

time: 229 us -> 199 us (0.87)
  Pallas kernels: 214 us -> 185 us
    pallas_call x1, Pallas kernels: 214 us -> 185 us  [on_device(): pl.pallas_call(functools.partial(streamed, sizes, None), in_specs=[vmem]...]
where the time goes in v1:
time: 199 us
  Pallas kernels  185 us (93%)
  local copies, waits for them, and re-layouts  7.27 us (4%)
  other arithmetic  6.54 us (3%)
    pallas_call x1, Pallas kernels, on_device(): pl.pallas_call(functools.partial(streamed, sizes, None), in_specs=[vmem]...  185 us

profile of v1, /device:TPU:0, one launch (start us, length us, event | category | flops | bytes accessed | tf_op | source)
XLA Modules:
  0.0 198.9 jit_solution(16332905926511916670)
XLA Ops:
  0.0 0.7 exp.6
  0.7 0.9 cosine_multiply_fusion
  1.6 0.1 stack_reshape.21
  1.6 0.1 stack_reshape.22
  1.7 0.6 pad_maximum_fusion.2.a_ref
  2.3 1.0 convert_bitcast_fusion
  3.3 1.0 fusion
  4.3 1.1 subtract_convert_fusion
  5.4 0.0 copy-start.2
  5.4 0.8 pad_maximum_fusion.1.b_ref
  6.2 0.3 copy.41
  6.5 0.3 copy.40
  6.8 0.0 copy-start
  6.8 1.2 pad_maximum_fusion.c_ref
  8.0 0.0 copy-done.2
  8.0 0.0 copy-start.1
  8.0 0.1 reshape.37
  8.1 1.1 copy.45
  9.2 0.0 copy-done
  9.2 1.2 copy.38
  10.4 0.0 copy-done.1
  10.4 1.1 copy.39
  11.5 185.1 %streamed.1 = bf16[256,2048]{1,0:T(8,128)(2,1)} custom-call(bf16[4,512,128]{2,1,0:T(8,128)(2,1)} %bitcast.28, bf16[4,2,128,64]{3,2,1,0:T(8,128)(2,1)} %pad_maximum_fusion.1.b_ref, bf16[4,2,512,16]{3,2,1,0:T(8,128)(2,1)} %pad_maximum_fusion.c_ref, f32[4,2,512]{2,1,0:T(2,128)} %pad_maximum_fusion.2.a_ref, f32[4,1,128]{2,1,0:T(1,128)} %bitcast.35, ...), custom_call_target="tpu_custom_call" | custom-call | tf_op jit(solution)/shard_map/streamed/pallas_call | solution.py:874
  196.6 2.3 %copy.47 = bf16[256,2048]{1,0:T(8,128)(2,1)} copy(bf16[256,2048]{1,0:T(8,128)(2,1)} %streamed.1) | data formatting | bytes 2097152
Async XLA Ops:
  5.4 2.6 %copy-start.2 = (bf16[512,512]{1,0:T(8,128)(2,1)S(1)}, bf16[512,512]{1,0:T(8,128)(2,1)}, u32[]{:S(2)}) copy-start(bf16[512,512]{1,0:T(8,128)(2,1)} %param.15) | copy-start | bytes 1572868
  6.8 2.5 %copy-start = (bf16[128,2816]{1,0:T(8,128)(2,1)S(1)}, bf16[128,2816]{1,0:T(8,128)(2,1)}, u32[]{:S(2)}) copy-start(bf16[128,2816]{1,0:T(8,128)(2,1)} %param.27) | copy-start | bytes 2162692
  8.0 2.5 %copy-start.1 = (bf16[128,2816]{1,0:T(8,128)(2,1)S(1)}, bf16[128,2816]{1,0:T(8,128)(2,1)}, u32[]{:S(2)}) copy-start(bf16[128,2816]{1,0:T(8,128)(2,1)} %param.28) | copy-start | bytes 2162692

commit v2 on v1

--- a/solution.py
+++ b/solution.py
@@ -372,14 +372,16 @@
     return sent + peer_copies
 
 
-def streamed(sizes, scopes, x_ref, b_ref, c_ref, a_ref, k_ref, wo_ref, res_ref, gain_ref, gate_ref,
-             up_ref, down_ref, out_ref, *rest):
-    quarters, weights, rest = (gate_ref, up_ref, down_ref), rest[:3], rest[3:]
+def streamed(sizes, x_hbm, residual_hbm, decay_re, decay_im, log_step, in_re, in_im, out_re, out_im,
+             skip_hbm, wo_hbm, gain_hbm, gate_hbm, up_hbm, down_hbm, out_ref, *rest):
+    weights, rest = rest[:3], rest[3:]
     (extra, rows_ref, carried_ref, gates, hidden, partners, firsts, seconds, work, read_in,
-     read_out, ends, total, gathered, act, share, others, send_sem, recv_sem, local_sem) = rest
+     read_out, ends, total, gathered, prefix, plane_total, planes, turn, act, share, others,
+     x_raw, x_ref, res_ref, dr_ref, di_ref, ls_ref, inr_ref, ini_ref, outr_ref, outi_ref, k_ref,
+     wo_ref, gain_ref, raw, turned, down_ref, a_ref, ratio, send_sem, recv_sem, local_sem, load_sem) = rest
     blocks, rows, cb = x_ref.shape
     sb = a_ref.shape[2]
-    depth = gate_ref.shape[2]
+    slab, depth = weights[0].shape[0], raw.shape[1]
     width = wo_ref.shape[1]
     keep_rows = rows // 2
     span = rows // CHUNKS
@@ -389,10 +391,12 @@
     oh, ou, om, ov = 1 - h, 1 - u, 1 - m, 1 - v
     index = lambda h, u, m, v: ((h * 2 + u) * nm + m) * 2 + v
     me = index(h, u, m, v)
-    inner = u != h
     to_x, to_z, to_y = (h, u, m, ov, core), (h, ou, m, v, core), (h, u, om, v, core)
     to_c, to_b, to_t = (oh, u, m, v, core), (oh, ou, m, v, core), (h, u, m, v, 1 - core)
-    plane = [(a, b, c) for a in (h, oh) for b in (u, ou) for c in (v, ov)]
+    plane = [(h, b, c) for b in (u, ou) for c in (v, ov)]
+    plane += [(oh, b, c) for b in (h, oh) for c in (v, ov)]
+    is_inner = lax.rem(h + u, 2)
+    inner = is_inner == 1
     across = (((1,), (1,)), ((), ()))
     slots, everywhere, inside, moves = {}, [], [], []
     counter = iter(range(send_sem.shape[0]))
@@ -403,7 +407,7 @@
     def describe(src, dst, device, name, number):
         return pltpu.make_async_remote_copy(
             src_ref=src, dst_ref=dst, send_sem=send_sem.at[number],
-            recv_sem=recv_sem.at[slot(name)], device_id=device, device_id_type=MESH,
+            recv_sem=recv_sem.at[slot(name) if isinstance(name, tuple) else name], device_id=device, device_id_type=MESH,
         )
 
     def send(src, dst, device, name, kept=everywhere):
@@ -423,7 +427,8 @@
         return place(w, index(a, b, row, c))
 
     def mine(w, b, c):
-        return quarters[w].at[b * 2 + c]
+        at = pl.ds(pl.multiple_of((b * 2 + c) * slab, slab), slab)
+        return down_ref.at[at, :] if w == 2 else turned.at[w, at, :]
 
     def own(w):
         return mine(w, u, v)
@@ -438,13 +443,14 @@
         send(extra.at[w] if s else mine(w, ou, v), spot(w, s), to_z, ("z", w, s))
 
     def send_c(w, s):
-        send(spot(w, 1) if s else own(w), spot(w, s), to_c, ("cs", w, s))
+        early, late = slot(("e", w, s)), slot(("l", w, s))
+        send(spot(w, 1) if s else own(w), spot(w, s), to_c, late + is_inner * (early - late))
 
     def send_b(w, s):
-        send(extra.at[w] if s else mine(w, ou, v), spot(w, s), to_b, ("co", w, s), inside)
+        send(extra.at[w] if s else mine(w, ou, v), spot(w, s), to_b, ("e", w, s), inside)
 
     def relay(w, s):
-        send(spot(w, 2 + s), spot(w, 2 + s), to_c, ("co", w, s), inside)
+        send(spot(w, 2 + s), spot(w, 2 + s), to_c, ("l", w, s), inside)
 
     def send_y(w, j):
         send(own(w) if j == 0 else spot(w, j), spot(w, j), to_y, ("y", w, j))
@@ -458,11 +464,11 @@
     def wait_z(w, s):
         arrive(spot(w, 2 + s), to_z, ("z", w, s))
 
-    def wait_cs(w, s):
-        arrive(spot(w, 4 + s), to_c, ("cs", w, s))
-
-    def wait_co(w, s):
-        arrive(spot(w, 6 + s), to_c, ("co", w, s))
+    def wait_e(w, s):
+        arrive(spot(w, 4 + s), to_c, ("e", w, s))
+
+    def wait_l(w, s):
+        arrive(spot(w, 6 + s), to_c, ("l", w, s))
 
     def wait_y(w, j):
         arrive(spot(w, j, om), to_y, ("y", w, j))
@@ -476,16 +482,77 @@
         others_sp.append(there)
         pl.semaphore_signal(barrier, inc=1, device_id=there, device_id_type=MESH)
     pl.semaphore_signal(barrier, inc=1, device_id=to_t, device_id_type=MESH)
+    pairs = ((gate_hbm, raw.at[0]), (up_hbm, raw.at[1]), (decay_re, dr_ref), (decay_im, di_ref),
+             (log_step, ls_ref), (x_hbm, x_raw), (in_re, inr_ref), (in_im, ini_ref),
+             (out_re, outr_ref), (out_im, outi_ref), (down_hbm, down_ref), (skip_hbm, k_ref),
+             (wo_hbm, wo_ref), (residual_hbm, res_ref), (gain_hbm, gain_ref))
+    loads = [pltpu.make_async_copy(a, b, load_sem.at[i]) for i, (a, b) in enumerate(pairs)]
+    for copy in loads:
+        copy.start()
+    exact = lax.Precision.HIGHEST
+
+    def flip_weights(w):
+        for i in range(raw.shape[2] // depth):
+            turned[w, i * depth:(i + 1) * depth, :] = raw[w, :, i * depth:(i + 1) * depth].T
+
+    with jax.named_scope("A_flip"):
+        loads[0].wait()
+        flip_weights(0)
+    with jax.named_scope("A_param"):
+        for copy in loads[2:5]:
+            copy.wait()
+        states = sb // GATHER
+        spread = (lax.rem(iota((states, sb), 1), states) == iota((states, sb), 0)).astype(F32)
+        chosen = lax.div(iota((GATHER, sb), 1), states) == iota((GATHER, sb), 0)
+        for b in range(blocks):
+            def lanes(ref):
+                wide = jnp.dot(ref[b * GATHER:(b + 1) * GATHER, :], spread, precision=exact,
+                               preferred_element_type=F32)
+                return jnp.sum(jnp.where(chosen, wide, 0.0), axis=0, keepdims=True)
+
+            groups = ls_ref.shape[1]
+            group = (lax.div(iota((groups, sb), 1), states) + b * GATHER
+                     == iota((groups, sb), 0)).astype(F32)
+            step_size = jnp.exp(jnp.dot(ls_ref[...], group, precision=exact,
+                                        preferred_element_type=F32))
+            re, im = lanes(dr_ref), lanes(di_ref)
+            magnitude = jnp.exp(re * step_size)
+            angle = im * step_size
+            power_re = magnitude * jnp.cos(angle)
+            power_im = magnitude * jnp.sin(angle)
+            denom = re * re + im * im
+            a_ref[b, 0:1, :] = power_re
+            a_ref[b, 1:2, :] = power_im
+            ratio[b, 0:1, :] = ((power_re - 1.0) * re + power_im * im) / denom
+            ratio[b, 1:2, :] = (power_im * re - (power_re - 1.0) * im) / denom
+    with jax.named_scope("A_x"):
+        square = (rows, rows)
+        source = lax.rem(iota(square, 0), span) * CHUNKS + lax.div(iota(square, 0), span)
+        turn[...] = (iota(square, 1) == source).astype(BF16)
+        loads[5].wait()
+        for b in range(blocks):
+            x_ref[b] = lax.dot_general(
+                turn[...], x_raw[:, b * cb:(b + 1) * cb], (((0,), (0,)), ((), ())),
+                preferred_element_type=F32,
+            ).astype(BF16)
     with jax.named_scope("A_barrier"):
         pl.semaphore_wait(barrier, n)
-
-    send_x(0, 0)
+    loads[10].wait()
+
+    def send_inner(w, s):
+        @pl.when(inner)
+        def _():
+            send_b(w, s)
+
+    send_x(0, 1)
     send_z(0, 0)
     send_y(0, 0)
-
-    @pl.when(inner)
-    def _():
-        send_b(0, 0)
+    send_inner(0, 0)
+    with jax.named_scope("A_flip1"):
+        loads[1].wait()
+        flip_weights(1)
+        for copy in loads[6:10]:
+            copy.wait()
 
     local = []
     for w in range(3):
@@ -509,17 +576,17 @@
 
         return lax.fori_loop(0, span, step, start, unroll=8)
 
+    size = cb // GATHER
     with jax.named_scope("B_scan1"):
         @pl.loop(0, blocks)
         def _(b):
-            states = b_ref.shape[3]
-            for half in range(2):
-                read_in[b, :, half * sb:(half + 1) * sb] = tiled(
-                    b_ref[b, half], GATHER, states, cb // GATHER
-                )
-                read_out[b, half * sb:(half + 1) * sb, :] = tiled(
-                    c_ref[b, half], GATHER, cb // GATHER, states
-                )
+            keep = lax.div(iota((cb, sb), 0), size) == lax.div(iota((cb, sb), 1), states)
+            at = pl.ds(pl.multiple_of(b * cb, cb), cb)
+            vr, vi = (jnp.dot(ref[at, :], spread, precision=exact, preferred_element_type=F32)
+                      for ref in (inr_ref, ini_ref))
+            cr, ci = ratio[b, 0:1, :], ratio[b, 1:2, :]
+            read_in[b, :, :sb] = jnp.where(keep, cr * vr - ci * vi, 0.0).astype(BF16)
+            read_in[b, :, sb:] = jnp.where(keep, cr * vi + ci * vr, 0.0).astype(BF16)
             zero = jnp.zeros((CHUNKS, sb), F32)
             sr, si = scan(b, (zero, zero), False)
             ends[b, :, :sb] = sr
@@ -532,61 +599,142 @@
             total[b, :, :sb] = er
             total[b, :, sb:] = ei
 
-    for k, there in enumerate(others_sp):
-        send(total, gathered.at[me], there, ("s", k))
-    gathered[me] = total[...]
-
-    send_x(0, 1)
+    here = m * 2 + v
+    level = h * 2 + u
+    for k, there in enumerate((to_x, to_y, (h, u, om, ov, core))):
+        send(total, gathered.at[here], there, ("s", k))
+    gathered[here] = total[...]
+    send_x(0, 0)
+    for w in (1, 2):
+        for s in (1, 0):
+            send_x(w, s)
+    send_y(1, 0)
+    send_y(2, 0)
+    with jax.named_scope("C_readout"):
+        @pl.loop(0, blocks)
+        def _(b):
+            high = (lax.rem(iota((sb, states), 0), states) == iota((sb, states), 1)).astype(BF16)
+            keep = lax.div(iota((sb, cb), 0), states) == lax.div(iota((sb, cb), 1), size)
+            at = pl.ds(pl.multiple_of(b * cb, cb), cb)
+            for place_in, ref, sign in ((0, outr_ref, 1.0), (1, outi_ref, -1.0)):
+                wide = lax.dot_general(high, (sign * ref[at, :]).astype(BF16), across,
+                                       preferred_element_type=F32)
+                read_out[b, place_in * sb:(place_in + 1) * sb, :] = jnp.where(
+                    keep, wide, 0.0).astype(BF16)
+
+    with jax.named_scope("C_states1"):
+        for k, (a, b) in enumerate(((m, ov), (om, v), (om, ov))):
+            arrive(gathered.at[a * 2 + b], to_x, ("s", k))
+
+    def power_of(b, count):
+        return cpow(a_ref[b, 0:1, :], a_ref[b, 1:2, :], count)
+
+    @pl.loop(0, blocks)
+    def _(b):
+        tr, ti = power_of(b, span * CHUNKS)
+        hr = jnp.zeros((1, sb), F32)
+        hi, pr, pi = hr, hr, hr
+        for device in range(4):
+            gr, gi = gathered[device, b, :, :sb], gathered[device, b, :, sb:]
+            nr, ni = cmul(tr, ti, hr, hi)
+            hr = jnp.where(device < here, nr + gr, hr)
+            hi = jnp.where(device < here, ni + gi, hi)
+            nr, ni = cmul(tr, ti, pr, pi)
+            pr, pi = nr + gr, ni + gi
+        prefix[b, :, :sb] = hr
+        prefix[b, :, sb:] = hi
+        plane_total[b, :, :sb] = pr
+        plane_total[b, :, sb:] = pi
+
+    for k, (a, b) in enumerate(((h, ou), (oh, u), (oh, ou))):
+        send(plane_total, planes.at[level], (a, b, m, v, core), ("plane", k))
+    planes[level] = plane_total[...]
+    with jax.named_scope("C_x01"):
+        wait_x(0, 1)
+    send_z(0, 1)
+    send_inner(0, 1)
     send_c(0, 0)
-    for w in (1, 2):
-        for s in range(2):
-            send_x(w, s)
-    with jax.named_scope("C_x0"):
+    for copy in loads[11:]:
+        copy.wait()
+    with jax.named_scope("C_states2"):
+        for k, (a, b) in enumerate(((h, ou), (oh, u), (oh, ou))):
+            arrive(planes.at[a * 2 + b], to_x, ("plane", k))
+    with jax.named_scope("C_x00"):
         wait_x(0, 0)
     send_c(0, 1)
     send_y(0, 1)
-    with jax.named_scope("C_states"):
-        for k in range(n - 1):
-            arrive(gathered.at[lax.rem(me + n - 1 - k, n)], others_sp[k], ("s", k))
-
-    square = (rows, rows)
-    source = lax.rem(iota(square, 0), span) * CHUNKS + lax.div(iota(square, 0), span)
-
-    with jax.named_scope("D_scan2"):
-        @pl.loop(0, blocks)
+
+    def second(b):
+        lr, li = power_of(b, span)
+        tr, ti = cpow(lr, li, CHUNKS)
+        qr, qi = cpow(tr, ti, 4)
+        hr = jnp.zeros((1, sb), F32)
+        hi = hr
+        for other in range(3):
+            nr, ni = cmul(qr, qi, hr, hi)
+            hr = jnp.where(other < level, nr + planes[other, b, :, :sb], hr)
+            hi = jnp.where(other < level, ni + planes[other, b, :, sb:], hi)
+        for device in range(3):
+            nr, ni = cmul(tr, ti, hr, hi)
+            hr, hi = jnp.where(device < here, nr, hr), jnp.where(device < here, ni, hi)
+        hr, hi = hr + prefix[b, :, :sb], hi + prefix[b, :, sb:]
+        starts_r, starts_i = [hr], [hi]
+        for chunk in range(CHUNKS - 1):
+            nr, ni = cmul(lr, li, hr, hi)
+            hr = nr + ends[b, chunk:chunk + 1, :sb]
+            hi = ni + ends[b, chunk:chunk + 1, sb:]
+            starts_r.append(hr)
+            starts_i.append(hi)
+        scan(b, (jnp.concatenate(starts_r, axis=0), jnp.concatenate(starts_i, axis=0)), True)
+        mixed = jnp.dot(work[...].astype(BF16), read_out[b], preferred_element_type=F32)
+        at = pl.ds(pl.multiple_of(b * cb, cb), cb)
+        mixed = mixed + k_ref[:, at] * x_ref[b].astype(F32)
+        mixed = jax.nn.gelu(mixed).astype(BF16)
+        act[:, at] = jnp.dot(
+            turn[...], mixed, preferred_element_type=F32
+        ).astype(BF16)
+
+    def pass_z(w, s):
+        with jax.named_scope(f"z{w}{s}"):
+            wait_z(w, s)
+
+        @pl.when(inner)
+        def _():
+            relay(w, s)
+
+        send_y(w, 2 + s)
+
+    def pass_e(w, s):
+        with jax.named_scope(f"e{w}{s}"):
+            wait_e(w, s)
+        send_y(w, 4 + s)
+
+    def pass_l(w, s):
+        with jax.named_scope(f"l{w}{s}"):
+            wait_l(w, s)
+        send_y(w, 6 + s)
+
+    with jax.named_scope("D_scan2a"):
+        @pl.loop(0, blocks // 2)
         def _(b):
-            lr, li = cpow(a_ref[b, 0:1, :], a_ref[b, 1:2, :], span)
-            tr, ti = cpow(lr, li, CHUNKS)
-            hr = jnp.zeros((1, sb), F32)
-            hi = hr
-            for device in range(n - 1):
-                nr, ni = cmul(tr, ti, hr, hi)
-                nr = nr + gathered[device, b, :, :sb]
-                ni = ni + gathered[device, b, :, sb:]
-                hr, hi = jnp.where(device < me, nr, hr), jnp.where(device < me, ni, hi)
-            starts_r, starts_i = [hr], [hi]
-            for chunk in range(CHUNKS - 1):
-                nr, ni = cmul(lr, li, hr, hi)
-                hr = nr + ends[b, chunk:chunk + 1, :sb]
-                hi = ni + ends[b, chunk:chunk + 1, sb:]
-                starts_r.append(hr)
-                starts_i.append(hi)
-            scan(b, (jnp.concatenate(starts_r, axis=0), jnp.concatenate(starts_i, axis=0)), True)
-            mixed = jnp.dot(work[...].astype(BF16), read_out[b], preferred_element_type=F32)
-            mixed = mixed + k_ref[b] * x_ref[b].astype(F32)
-            mixed = jax.nn.gelu(mixed).astype(BF16)
-            turn = (iota(square, 1) == source).astype(BF16)
-            act[:, pl.ds(pl.multiple_of(b * cb, cb), cb)] = jnp.dot(
-                turn, mixed, preferred_element_type=F32
-            ).astype(BF16)
-
-    with jax.named_scope("D_x1"):
-        wait_x(0, 1)
-    send_z(0, 1)
-
-    @pl.when(inner)
-    def _():
-        send_b(0, 1)
+            second(b)
+
+    pass_z(0, 0)
+    send_z(1, 0)
+    send_inner(1, 0)
+    with jax.named_scope("D_scan2b"):
+        @pl.loop(blocks // 2, blocks)
+        def _(b):
+            second(b)
+
+    pass_z(0, 1)
+    with jax.named_scope("D_x11"):
+        wait_x(1, 1)
+    send_z(1, 1)
+    send_inner(1, 1)
+    with jax.named_scope("D_x10"):
+        wait_x(1, 0)
+    send_y(1, 1)
 
     tile = min(512, width)
     with jax.named_scope("E_outproj"):
@@ -618,7 +766,9 @@
             rows_ref[0, 0, at, :] = (carried * scale * gain_ref[...]).astype(BF16)
 
     send(rows_ref.at[0, 0], rows_ref.at[0, 1], to_x, ("r", 1), moves)
-    send(rows_ref.at[0, 0], rows_ref.at[0, 2], to_z, ("r", 2), moves)
+    for part in range(2):
+        at = pl.ds(part * (keep_rows // 2), keep_rows // 2)
+        send(rows_ref.at[0, 0, at], rows_ref.at[0, 2, at], to_z, ("r", 2, part), moves)
     send(rows_ref.at[0, 0], rows_ref.at[1, 0], to_t, ("t", 0), moves)
 
     def share_core(k):
@@ -626,48 +776,6 @@
 
     def wait_core(k):
         arrive(rows_ref.at[1, k], to_t, ("t", k))
-
-    def own_blocks(w):
-        send_z(w, 0)
-        send_c(w, 0)
-        send_y(w, 0)
-
-        @pl.when(inner)
-        def _():
-            send_b(w, 0)
-
-        wait_x(w, 0)
-        send_c(w, 1)
-        send_y(w, 1)
-        wait_x(w, 1)
-        send_z(w, 1)
-
-        @pl.when(inner)
-        def _():
-            send_b(w, 1)
-
-    def pass_z(w):
-        for s in range(2):
-            with jax.named_scope(f"z{w}{s}"):
-                wait_z(w, s)
-
-            @pl.when(inner)
-            def _():
-                relay(w, s)
-
-            send_y(w, 2 + s)
-
-    def pass_c(w):
-        for s in range(2):
-            with jax.named_scope(f"cs{w}{s}"):
-                wait_cs(w, s)
-            send_y(w, 4 + s)
-
-    def pass_o(w):
-        for s in range(2):
-            with jax.named_scope(f"co{w}{s}"):
-                wait_co(w, s)
-            send_y(w, 6 + s)
 
     def gate_part(t, k):
         with jax.named_scope(f"gate{t}{k}"):
@@ -685,60 +793,94 @@
             ).astype(BF16)
 
     half = keep_rows // 2
-    with jax.named_scope("own1"):
-        own_blocks(1)
-    pass_z(0)
-    pass_c(0)
-    pass_o(0)
-    with jax.named_scope("r1"):
-        arrive(rows_ref.at[0, 1], to_x, ("r", 1))
-    send(rows_ref.at[0, 1, pl.ds(0, half)], rows_ref.at[0, 3, pl.ds(0, half)], to_z,
-         ("r", 3, 0), moves)
-    share_core(1)
-    with jax.named_scope("r2"):
-        arrive(rows_ref.at[0, 2], to_z, ("r", 2))
-    send(rows_ref.at[0, 2, pl.ds(half, half)], rows_ref.at[0, 3, pl.ds(half, half)], to_x,
-         ("r", 3, 1), moves)
-    share_core(2)
+
+    def first_rows():
+        with jax.named_scope("r1"):
+            arrive(rows_ref.at[0, 1], to_x, ("r", 1))
+        share_core(1)
+
+    def relay_rows(part):
+        at = pl.ds(part * half, half)
+        with jax.named_scope(f"r2{part}"):
+            arrive(rows_ref.at[0, 2, at], to_z, ("r", 2, part))
+        send(rows_ref.at[0, 2, at], rows_ref.at[0, 3, at], to_x, ("r", 3, part), moves)
+        if part:
+            share_core(2)
+
+    def last_rows():
+        with jax.named_scope("r3"):
+            for part in range(2):
+                at = pl.ds(part * half, half)
+                arrive(rows_ref.at[0, 3, at], to_x, ("r", 3, part))
+        share_core(3)
+
+    def second_weights():
+        send_z(2, 0)
+        send_inner(2, 0)
+        send_c(2, 0)
+        wait_x(2, 1)
+        send_z(2, 1)
+        send_inner(2, 1)
+        wait_x(2, 0)
+        send_y(2, 1)
+        send_c(2, 1)
+
+    def whole(w):
+        with jax.named_scope(f"y{w}"):
+            for j in range(8):
+                wait_y(w, j)
+
+    def core_rows(k):
+        with jax.named_scope(f"t{k}"):
+            wait_core(k)
+
+    send_c(1, 0)
+    send_c(1, 1)
+    pass_e(0, 0)
+    pass_e(0, 1)
+    pass_z(1, 0)
+    pass_z(1, 1)
+    pass_l(0, 0)
+    pass_l(0, 1)
+    pass_e(1, 0)
     for copy in local:
         copy.wait()
-    with jax.named_scope("y0"):
-        for j in range(8):
-            wait_y(0, j)
-    wait_core(0)
+    whole(0)
+    core_rows(0)
     gate_part(0, 0)
     gate_part(1, 0)
-    pass_z(1)
-    with jax.named_scope("own2"):
-        own_blocks(2)
+    pass_e(1, 1)
+    first_rows()
+    relay_rows(0)
     gate_part(0, 1)
-    wait_core(1)
+    second_weights()
+    core_rows(1)
     gate_part(1, 1)
-    pass_c(1)
+    pass_l(1, 0)
+    pass_l(1, 1)
+    relay_rows(1)
     gate_part(0, 2)
-    wait_core(2)
+    core_rows(2)
     gate_part(1, 2)
-    pass_o(1)
-    with jax.named_scope("r3"):
-        arrive(rows_ref.at[0, 3, pl.ds(0, half)], to_z, ("r", 3, 0))
-        arrive(rows_ref.at[0, 3, pl.ds(half, half)], to_x, ("r", 3, 1))
-    share_core(3)
+    pass_z(2, 0)
+    pass_e(2, 0)
+    last_rows()
     gate_part(0, 3)
-    pass_z(2)
-    with jax.named_scope("t3"):
-        wait_core(3)
+    whole(1)
+    up_part(0, 1)
+    up_part(1, 1)
+    core_rows(3)
     gate_part(1, 3)
-    with jax.named_scope("y1"):
-        for j in range(8):
-            wait_y(1, j)
-    for t, k in ((0, 0), (1, 0), (0, 1)):
-        up_part(t, k)
-    pass_c(2)
-    for t, k in ((1, 1), (0, 2), (1, 2)):
-        up_part(t, k)
-    pass_o(2)
-    for t, k in ((0, 3), (1, 3)):
-        up_part(t, k)
+    up_part(0, 3)
+    up_part(1, 3)
+    pass_z(2, 1)
+    pass_e(2, 1)
+    up_part(0, 2)
+    up_part(1, 2)
+    pass_l(2, 0)
+    up_part(0, 0)
+    up_part(1, 0)
+    pass_l(2, 1)
     with jax.named_scope("moves"):
         for copy in moves:
             copy.wait_send()
@@ -854,26 +996,12 @@
     groups, states = decay_real.shape
     blocks = groups // GATHER
     cb, sb = channels // blocks, GATHER * states
-    power_re, power_im, bar_re, bar_im = discrete(
-        decay_real, decay_imag, log_step, in_real, in_imag
-    )
-    rows_first = lambda t: jnp.transpose(t, (0, 2, 1)).reshape(blocks, -1, t.shape[1])
-    read_in = jnp.stack([rows_first(bar_re), rows_first(bar_im)], axis=1).astype(BF16)
-    read_out = jnp.stack(
-        [rows_first(output_real), -rows_first(output_imaginary)], axis=1
-    ).astype(BF16)
-    power = jnp.stack([power_re.reshape(blocks, sb), power_im.reshape(blocks, sb)], axis=1)
-    x = mixer_in.reshape(CHUNKS, rows // CHUNKS, blocks, cb).transpose(2, 1, 0, 3)
-    x = x.reshape(blocks, rows, cb)
     vmem = pl.BlockSpec(memory_space=pltpu.VMEM)
-    operands = (x, read_in, read_out, power, skip.reshape(blocks, 1, cb), out_proj, residual,
-                norm_gain.reshape(1, width), w_gate.T.reshape(4, part, depth),
-                w_up.T.reshape(4, part, depth), w_down.reshape(4, part, depth))
     if depth % 128 == 0 and (tp, nh, nm) == (2, 2, 2):
         cut = width // 8
         return pl.pallas_call(
-            functools.partial(streamed, sizes, None),
-            in_specs=[vmem] * 11,
+            functools.partial(streamed, sizes),
+            in_specs=[pl.BlockSpec(memory_space=pl.ANY)] * 15,
             out_specs=vmem,
             out_shape=jax.ShapeDtypeStruct((keep_rows, width), BF16),
             scratch_shapes=[
@@ -891,19 +1019,56 @@
                 pltpu.VMEM((blocks, 2 * sb, cb), BF16),
                 pltpu.VMEM((blocks, CHUNKS, 2 * sb), F32),
                 pltpu.VMEM((blocks, 1, 2 * sb), F32),
-                pltpu.VMEM((n, blocks, 1, 2 * sb), F32),
+                pltpu.VMEM((4, blocks, 1, 2 * sb), F32),
+                pltpu.VMEM((blocks, 1, 2 * sb), F32),
+                pltpu.VMEM((blocks, 1, 2 * sb), F32),
+                pltpu.VMEM((4, blocks, 1, 2 * sb), F32),
+                pltpu.VMEM((rows, rows), BF16),
                 pltpu.VMEM((rows, channels), BF16),
                 pltpu.VMEM((2, keep_rows, width), BF16),
                 pltpu.VMEM((keep_rows, width), BF16),
+                pltpu.VMEM((rows, channels), BF16),
+                pltpu.VMEM((blocks, rows, cb), BF16),
+                pltpu.VMEM((keep_rows, width), BF16),
+                *[pltpu.VMEM((groups, states), F32)] * 2,
+                pltpu.VMEM((1, groups), F32),
+                *[pltpu.VMEM((channels, states), F32)] * 4,
+                pltpu.VMEM((1, channels), F32),
+                pltpu.VMEM((channels, width), BF16),
+                pltpu.VMEM((1, width), F32),
+                pltpu.VMEM((2, depth, hidden_units), BF16),
+                pltpu.VMEM((2, hidden_units, depth), BF16),
+                pltpu.VMEM((hidden_units, depth), BF16),
+                pltpu.VMEM((blocks, 2, sb), F32),
+                pltpu.VMEM((blocks, 2, sb), F32),
                 pltpu.SemaphoreType.DMA((160,)),
                 pltpu.SemaphoreType.DMA((160,)),
                 pltpu.SemaphoreType.DMA((3,)),
+                pltpu.SemaphoreType.DMA((15,)),
             ],
             compiler_params=pltpu.CompilerParams(
                 collective_id=0, has_side_effects=True, vmem_limit_bytes=62 * 2**20
             ),
             name="streamed",
-        )(*operands)
+        )(mixer_in, residual, decay_real, decay_imag, log_step.reshape(1, groups),
+          in_real.transpose(0, 2, 1).reshape(channels, states),
+          in_imag.transpose(0, 2, 1).reshape(channels, states),
+          output_real.reshape(channels, states), output_imaginary.reshape(channels, states),
+          skip.reshape(1, channels), out_proj, norm_gain.reshape(1, width), w_gate, w_up, w_down)
+    power_re, power_im, bar_re, bar_im = discrete(
+        decay_real, decay_imag, log_step, in_real, in_imag
+    )
+    rows_first = lambda t: jnp.transpose(t, (0, 2, 1)).reshape(blocks, -1, t.shape[1])
+    read_in = jnp.stack([rows_first(bar_re), rows_first(bar_im)], axis=1).astype(BF16)
+    read_out = jnp.stack(
+        [rows_first(output_real), -rows_first(output_imaginary)], axis=1
+    ).astype(BF16)
+    power = jnp.stack([power_re.reshape(blocks, sb), power_im.reshape(blocks, sb)], axis=1)
+    x = mixer_in.reshape(CHUNKS, rows // CHUNKS, blocks, cb).transpose(2, 1, 0, 3)
+    x = x.reshape(blocks, rows, cb)
+    operands = (x, read_in, read_out, power, skip.reshape(blocks, 1, cb), out_proj, residual,
+                norm_gain.reshape(1, width), w_gate.T.reshape(4, part, depth),
+                w_up.T.reshape(4, part, depth), w_down.reshape(4, part, depth))
     copies = 3 * (3 + 4 * (nh - 1) + 4 * nh * (nm - 1)) + (n - 1) + (tp - 1) + 3 + 4 * (tp - 1)
     laid = (part, n * depth) if depth % 128 == 0 else (n, part, depth)
     between = [(laid, BF16)] * 3 + [

time: 199 us -> 158 us (0.79)
  Pallas kernels: 185 us -> 155 us
  other arithmetic: 6.54 us -> 0 us
  local copies, waits for them, and re-layouts: 7.27 us -> 2.3 us
    pallas_call x1, Pallas kernels: 185 us -> 155 us  [on_device(): pl.pallas_call(functools.partial(streamed, sizes), in_specs=[pl.BlockSpec...]
    another operation x4 -> x0, other arithmetic: 3.7 us -> none  [the longest x1 1.18 us: on_device(): jnp.stack([rows_first(output_real), -rows_first(output_imaginary)], axis=1)]
    transpose x2 -> x0, local copies, waits for them, and re-layouts: 2.31 us -> none  [the longest x1 1.17 us: on_device(): w_gate.T.reshape(4, part, depth)]
where the time goes in v2:
time: 158 us
  Pallas kernels  155 us (98%)
  local copies, waits for them, and re-layouts  2.3 us (1%)
    pallas_call x1, Pallas kernels, on_device(): pl.pallas_call(functools.partial(streamed, sizes), in_specs=[pl.BlockSpec...  155 us

profile of v2, /device:TPU:0, one launch (start us, length us, event | category | flops | bytes accessed | tf_op | source)
XLA Modules:
  0.0 157.7 jit_solution(16793575923655328424)
XLA Ops:
  0.0 155.4 %streamed.1 = bf16[256,2048]{1,0:T(8,128)(2,1)} custom-call(bf16[512,512]{1,0:T(8,128)(2,1)} %x_hbm.1, bf16[256,2048]{1,0:T(8,128)(2,1)} %residual_hbm.1, f32[32,64]{1,0:T(8,128)} %decay_re.1, f32[32,64]{1,0:T(8,128)} %decay_im.1, f32[1,32]{1,0:T(1,128)} %bitcast.17, f32[512,64]{1,0:T(8,128)} %bitcast.11, f32[512,64]{1,0:T(8,128)} %bitcast.12, ...), custom_call_target="tpu_custom_call" | custom-call | tf_op jit(solution)/shard_map/streamed/pallas_call | solution.py:1002
  155.4 2.3 %copy.17 = bf16[256,2048]{1,0:T(8,128)(2,1)} copy(bf16[256,2048]{1,0:T(8,128)(2,1)} %streamed.1) | data formatting | bytes 2097152

commit v3 on v2

--- a/solution.py
+++ b/solution.py
@@ -14,6 +14,8 @@
 PEERS = ("u", "v")
 GATHER = 8
 CHUNKS = 8
+X_FIRST = (1, 0, 1, 0, 1, 0, 1, 0)
+PIECES = 4
 MESH = pl.DeviceIdType.MESH
 
 
@@ -442,9 +444,18 @@
     def send_z(w, s):
         send(extra.at[w] if s else mine(w, ou, v), spot(w, s), to_z, ("z", w, s))
 
-    def send_c(w, s):
-        early, late = slot(("e", w, s)), slot(("l", w, s))
-        send(spot(w, 1) if s else own(w), spot(w, s), to_c, late + is_inner * (early - late))
+    numbers = {}
+
+    def send_c(w, s, kind):
+        number = numbers.setdefault((w, s), None) or next(counter)
+        if numbers[w, s] is None:
+            numbers[w, s] = number
+            everywhere.append(describe(extra.at[0], extra.at[0], to_c, ("e", w, s), number))
+        name = ("e" if kind else "l", w, s)
+
+        @pl.when(is_inner == kind)
+        def _():
+            describe(spot(w, 1) if s else own(w), spot(w, s), to_c, name, number).start()
 
     def send_b(w, s):
         send(extra.at[w] if s else mine(w, ou, v), spot(w, s), to_b, ("e", w, s), inside)
@@ -548,6 +559,7 @@
     send_z(0, 0)
     send_y(0, 0)
     send_inner(0, 0)
+    send_c(0, 0, 1)
     with jax.named_scope("A_flip1"):
         loads[1].wait()
         flip_weights(1)
@@ -577,13 +589,19 @@
         return lax.fori_loop(0, span, step, start, unroll=8)
 
     size = cb // GATHER
+    spread_narrow = spread.astype(BF16)
     with jax.named_scope("B_scan1"):
         @pl.loop(0, blocks)
         def _(b):
             keep = lax.div(iota((cb, sb), 0), size) == lax.div(iota((cb, sb), 1), states)
             at = pl.ds(pl.multiple_of(b * cb, cb), cb)
-            vr, vi = (jnp.dot(ref[at, :], spread, precision=exact, preferred_element_type=F32)
-                      for ref in (inr_ref, ini_ref))
+            def widen(ref):
+                high = ref[at, :].astype(BF16)
+                low = (ref[at, :] - high.astype(F32)).astype(BF16)
+                return (jnp.dot(high, spread_narrow, preferred_element_type=F32)
+                        + jnp.dot(low, spread_narrow, preferred_element_type=F32))
+
+            vr, vi = widen(inr_ref), widen(ini_ref)
             cr, ci = ratio[b, 0:1, :], ratio[b, 1:2, :]
             read_in[b, :, :sb] = jnp.where(keep, cr * vr - ci * vi, 0.0).astype(BF16)
             read_in[b, :, sb:] = jnp.where(keep, cr * vi + ci * vr, 0.0).astype(BF16)
@@ -653,7 +671,7 @@
         wait_x(0, 1)
     send_z(0, 1)
     send_inner(0, 1)
-    send_c(0, 0)
+    send_c(0, 0, 0)
     for copy in loads[11:]:
         copy.wait()
     with jax.named_scope("C_states2"):
@@ -661,7 +679,8 @@
             arrive(planes.at[a * 2 + b], to_x, ("plane", k))
     with jax.named_scope("C_x00"):
         wait_x(0, 0)
-    send_c(0, 1)
+    send_c(0, 1, 0)
+    send_c(0, 1, 1)
     send_y(0, 1)
 
     def second(b):
@@ -766,8 +785,9 @@
             rows_ref[0, 0, at, :] = (carried * scale * gain_ref[...]).astype(BF16)
 
     send(rows_ref.at[0, 0], rows_ref.at[0, 1], to_x, ("r", 1), moves)
-    for part in range(2):
-        at = pl.ds(part * (keep_rows // 2), keep_rows // 2)
+    piece = keep_rows // PIECES
+    for part in range(PIECES):
+        at = pl.ds(part * piece, piece)
         send(rows_ref.at[0, 0, at], rows_ref.at[0, 2, at], to_z, ("r", 2, part), moves)
     send(rows_ref.at[0, 0], rows_ref.at[1, 0], to_t, ("t", 0), moves)
 
@@ -777,22 +797,20 @@
     def wait_core(k):
         arrive(rows_ref.at[1, k], to_t, ("t", k))
 
-    def gate_part(t, k):
-        with jax.named_scope(f"gate{t}{k}"):
-            gates[4 * t + k] = lax.dot_general(
-                rows_ref[t, k], weights[0][...], across, preferred_element_type=F32
-            )
-
-    def up_part(t, k):
-        with jax.named_scope(f"up{t}{k}"):
-            up = lax.dot_general(
-                rows_ref[t, k], weights[1][...], across, preferred_element_type=F32
-            )
-            hidden[pl.ds((4 * t + k) * keep_rows, keep_rows), :] = (
-                jax.nn.silu(gates[4 * t + k]) * up
-            ).astype(BF16)
-
-    half = keep_rows // 2
+    def product(k, w):
+        block = rows_ref[:, k].reshape(2 * keep_rows, width)
+        return lax.dot_general(block, weights[w][...], across, preferred_element_type=F32)
+
+    def gate_part(k):
+        with jax.named_scope(f"gate{k}"):
+            gates[k] = product(k, 0)
+
+    def up_part(k):
+        with jax.named_scope(f"up{k}"):
+            result = (jax.nn.silu(gates[k]) * product(k, 1)).astype(BF16)
+            for t in range(2):
+                hidden[pl.ds((4 * t + k) * keep_rows, keep_rows), :] = (
+                    result[t * keep_rows:(t + 1) * keep_rows])
 
     def first_rows():
         with jax.named_scope("r1"):
@@ -800,30 +818,34 @@
         share_core(1)
 
     def relay_rows(part):
-        at = pl.ds(part * half, half)
+        at = pl.ds(part * piece, piece)
         with jax.named_scope(f"r2{part}"):
             arrive(rows_ref.at[0, 2, at], to_z, ("r", 2, part))
         send(rows_ref.at[0, 2, at], rows_ref.at[0, 3, at], to_x, ("r", 3, part), moves)
-        if part:
+        if part == PIECES - 1:
             share_core(2)
 
     def last_rows():
         with jax.named_scope("r3"):
-            for part in range(2):
-                at = pl.ds(part * half, half)
+            for part in range(PIECES):
+                at = pl.ds(part * piece, piece)
                 arrive(rows_ref.at[0, 3, at], to_x, ("r", 3, part))
         share_core(3)
 
     def second_weights():
+        send_inner(2, 0)
+        wait_x(2, 1)
+        send_inner(2, 1)
         send_z(2, 0)
-        send_inner(2, 0)
-        send_c(2, 0)
-        wait_x(2, 1)
         send_z(2, 1)
-        send_inner(2, 1)
         wait_x(2, 0)
         send_y(2, 1)
-        send_c(2, 1)
+        send_c(2, 0, 0)
+        send_c(2, 1, 0)
+
+    def delayed_weights():
+        send_c(2, 0, 1)
+        send_c(2, 1, 1)
 
     def whole(w):
         with jax.named_scope(f"y{w}"):
@@ -834,8 +856,9 @@
         with jax.named_scope(f"t{k}"):
             wait_core(k)
 
-    send_c(1, 0)
-    send_c(1, 1)
+    for s in range(2):
+        send_c(1, s, 1)
+        send_c(1, s, 0)
     pass_e(0, 0)
     pass_e(0, 1)
     pass_z(1, 0)
@@ -847,46 +870,38 @@
         copy.wait()
     whole(0)
     core_rows(0)
-    gate_part(0, 0)
-    gate_part(1, 0)
+    gate_part(0)
+    first_rows()
+    second_weights()
+    relay_rows(0)
     pass_e(1, 1)
-    first_rows()
-    relay_rows(0)
-    gate_part(0, 1)
-    second_weights()
+    relay_rows(1)
     core_rows(1)
-    gate_part(1, 1)
+    gate_part(1)
     pass_l(1, 0)
     pass_l(1, 1)
-    relay_rows(1)
-    gate_part(0, 2)
+    delayed_weights()
+    relay_rows(2)
+    whole(1)
+    up_part(0)
+    relay_rows(3)
+    up_part(1)
     core_rows(2)
-    gate_part(1, 2)
+    gate_part(2)
     pass_z(2, 0)
+    last_rows()
+    up_part(2)
+    core_rows(3)
+    gate_part(3)
+    up_part(3)
     pass_e(2, 0)
-    last_rows()
-    gate_part(0, 3)
-    whole(1)
-    up_part(0, 1)
-    up_part(1, 1)
-    core_rows(3)
-    gate_part(1, 3)
-    up_part(0, 3)
-    up_part(1, 3)
-    pass_z(2, 1)
-    pass_e(2, 1)
-    up_part(0, 2)
-    up_part(1, 2)
-    pass_l(2, 0)
-    up_part(0, 0)
-    up_part(1, 0)
-    pass_l(2, 1)
     with jax.named_scope("moves"):
         for copy in moves:
             copy.wait_send()
 
     across_u = width // 8
-    chunks = [(a, b, c) for a in (h, oh) for c in (m, om) for b in range(2)]
+    chunks = [(h, h, m), (h, oh, m), (oh, h, m), (h, h, om), (h, oh, om), (oh, oh, m),
+              (oh, h, om), (oh, oh, om)]
 
     def columns(j):
         a, b, c = chunks[j]
@@ -916,8 +931,8 @@
 
     def pair(j):
         at = columns(j)
-        near, far = (1, 2) if j % 2 == 0 else (2, 1)
-        device = to_x if j % 2 == 0 else to_z
+        near, far = (1, 2) if X_FIRST[j] else (2, 1)
+        device = to_x if X_FIRST[j] else to_z
         arrive(partners.at[j], to_t, ("p", j))
         for place_in, k in enumerate((3, near)):
             add(k, j, partners.at[j, k])
@@ -927,8 +942,8 @@
 
     def combine(j):
         at = columns(j)
-        far = 2 if j % 2 == 0 else 1
-        device, other = (to_x, to_z) if j % 2 == 0 else (to_z, to_x)
+        far = 2 if X_FIRST[j] else 1
+        device, other = (to_x, to_z) if X_FIRST[j] else (to_z, to_x)
         arrive(firsts.at[j, 0], device, ("f", j, 0))
         add(far, j, firsts.at[j, 0])
         send(rows_ref.at[0, far, :, at], seconds.at[j], other, ("g", j))
@@ -937,7 +952,7 @@
 
     def finish(j):
         at = columns(j)
-        arrive(seconds.at[j], to_z if j % 2 == 0 else to_x, ("g", j))
+        arrive(seconds.at[j], to_z if X_FIRST[j] else to_x, ("g", j))
 
         @pl.loop(0, keep_rows // line)
         def _(i):
@@ -946,28 +961,42 @@
             summed = summed.astype(BF16).astype(F32)
             out_ref[lines, at] = (carried_ref[lines, at] + 0.5 * summed).astype(BF16)
 
-    lag = (1, 3, 5)
-    for step in range(8 + lag[2]):
-        if step < 8:
-            if step == 2:
-                with jax.named_scope("y2a"):
-                    for j in range(4):
-                        wait_y(2, j)
-            if step == 6:
-                with jax.named_scope("y2b"):
-                    for j in range(4, 8):
-                        wait_y(2, j)
-            with jax.named_scope(f"down{step}"):
-                down(step)
-        if 0 <= step - lag[0] < 8:
-            with jax.named_scope(f"pair{step - lag[0]}"):
-                pair(step - lag[0])
-        if 0 <= step - lag[1] < 8:
-            with jax.named_scope(f"comb{step - lag[1]}"):
-                combine(step - lag[1])
-        if 0 <= step - lag[2] < 8:
-            with jax.named_scope(f"fin{step - lag[2]}"):
-                finish(step - lag[2])
+    order = ("d0", "z", "p0", "d1", "e", "d2", "p1", "d3", "p2", "c0", "d4", "p3", "c1", "l", "d5",
+             "p4", "c2", "f0", "d6", "p5", "c3", "f1", "d7", "p6", "c4", "f2", "p7", "c5", "f3",
+             "c6", "f4", "c7", "f5", "f6", "f7")
+    relayed, passed = next(counter), next(counter)
+    inside.append((("l", 2, 1), relayed))
+    everywhere.append(describe(extra.at[0], extra.at[0], to_y, ("y", 2, 3), passed))
+
+    def late_z(kind):
+        @pl.when(is_inner == kind)
+        def _():
+            wait_z(2, 1)
+            if kind:
+                describe(spot(2, 3), spot(2, 3), to_c, ("l", 2, 1), relayed).start()
+            describe(spot(2, 3), spot(2, 3), to_y, ("y", 2, 3), passed).start()
+
+    with jax.named_scope("z21"):
+        late_z(1)
+    stages = {"d": down, "p": pair, "c": combine, "f": finish}
+    for word in order:
+        if word == "z":
+            late_z(0)
+            continue
+        if word == "e":
+            pass_e(2, 1)
+            continue
+        if word == "l":
+            pass_l(2, 0)
+            pass_l(2, 1)
+            continue
+        j = int(word[1])
+        if word in ("d3", "d6", "d7"):
+            with jax.named_scope("y2" + word):
+                for i in {"d3": (0, 1, 2, 3), "d6": (4, 5), "d7": (6, 7)}[word]:
+                    wait_y(2, i)
+        with jax.named_scope({"d": "down", "p": "pair", "c": "comb", "f": "fin"}[word[0]] + word[1]):
+            stages[word[0]](j)
     for copy in everywhere:
         copy.wait_send()
 
@@ -1009,7 +1038,7 @@
                 pltpu.VMEM((3, part, depth), BF16),
                 pltpu.VMEM((2, 4, keep_rows, width), BF16),
                 pltpu.VMEM((keep_rows, width), F32),
-                pltpu.VMEM((8, keep_rows, part), F32),
+                pltpu.VMEM((4, 2 * keep_rows, part), F32),
                 pltpu.VMEM((8 * keep_rows, part), BF16),
                 pltpu.VMEM((8, 4, keep_rows, cut), BF16),
                 pltpu.VMEM((8, 2, keep_rows, cut), BF16),

time: 158 us -> 147 us (0.930)
  Pallas kernels: 155 us -> 145 us
    pallas_call x1, Pallas kernels: 155 us -> 145 us  [on_device(): pl.pallas_call(functools.partial(streamed, sizes), in_specs=[pl.BlockSpec...]
where the time goes in v3:
time: 147 us
  Pallas kernels  145 us (99%)
  local copies, waits for them, and re-layouts  2.3 us (2%)
    pallas_call x1, Pallas kernels, on_device(): pl.pallas_call(functools.partial(streamed, sizes), in_specs=[pl.BlockSpec...  145 us

profile of v3, /device:TPU:0, one launch (start us, length us, event | category | flops | bytes accessed | tf_op | source)
XLA Modules:
  0.0 147.1 jit_solution(7225815222913599060)
XLA Ops:
  0.0 144.8 %streamed.1 = bf16[256,2048]{1,0:T(8,128)(2,1)} custom-call(bf16[512,512]{1,0:T(8,128)(2,1)} %x_hbm.1, bf16[256,2048]{1,0:T(8,128)(2,1)} %residual_hbm.1, f32[32,64]{1,0:T(8,128)} %decay_re.1, f32[32,64]{1,0:T(8,128)} %decay_im.1, f32[1,32]{1,0:T(1,128)} %bitcast.17, f32[512,64]{1,0:T(8,128)} %bitcast.11, f32[512,64]{1,0:T(8,128)} %bitcast.12, ...), custom_call_target="tpu_custom_call" | custom-call | tf_op jit(solution)/shard_map/streamed/pallas_call | solution.py:1031
  144.8 2.3 %copy.17 = bf16[256,2048]{1,0:T(8,128)(2,1)} copy(bf16[256,2048]{1,0:T(8,128)(2,1)} %streamed.1) | data formatting | bytes 2097152

commit v4 on v3

--- a/solution.py
+++ b/solution.py
@@ -14,8 +14,10 @@
 PEERS = ("u", "v")
 GATHER = 8
 CHUNKS = 8
-X_FIRST = (1, 0, 1, 0, 1, 0, 1, 0)
+X_FIRST = (1, 1, 1, 0, 1, 0, 1, 0)
 PIECES = 4
+ORDER = ("d0", "e", "p0", "p1", "d1", "p2", "p3", "l", "d2", "p4", "p5", "c0", "d3", "p6", "p7",
+         "c1", "c2", "c3", "c4", "c5", "f0", "f1", "c6", "c7", "f2", "f3", "f4", "f5", "f6", "f7")
 MESH = pl.DeviceIdType.MESH
 
 
@@ -375,15 +377,15 @@
 
 
 def streamed(sizes, x_hbm, residual_hbm, decay_re, decay_im, log_step, in_re, in_im, out_re, out_im,
-             skip_hbm, wo_hbm, gain_hbm, gate_hbm, up_hbm, down_hbm, out_ref, *rest):
-    weights, rest = rest[:3], rest[3:]
-    (extra, rows_ref, carried_ref, gates, hidden, partners, firsts, seconds, work, read_in,
+             skip_hbm, wo_hbm, gain_hbm, gate_hbm, up_hbm, down_hbm, out_hbm, *rest):
+    (out_ref, out_sem, joined, down_full, extra, rows_ref, carried_ref, gates, hidden, partners, firsts, seconds, work, read_in,
      read_out, ends, total, gathered, prefix, plane_total, planes, turn, act, share, others,
      x_raw, x_ref, res_ref, dr_ref, di_ref, ls_ref, inr_ref, ini_ref, outr_ref, outi_ref, k_ref,
      wo_ref, gain_ref, raw, turned, down_ref, a_ref, ratio, send_sem, recv_sem, local_sem, load_sem) = rest
     blocks, rows, cb = x_ref.shape
     sb = a_ref.shape[2]
-    slab, depth = weights[0].shape[0], raw.shape[1]
+    slab, depth = down_full.shape[0], raw.shape[1]
+    pitch = joined.shape[0] // 2
     width = wo_ref.shape[1]
     keep_rows = rows // 2
     span = rows // CHUNKS
@@ -422,7 +424,8 @@
         describe(dst, dst, device, name, 0).wait_recv()
 
     def place(w, position):
-        return weights[w].at[:, pl.ds(pl.multiple_of(position * depth, depth), depth)]
+        at = pl.ds(pl.multiple_of(position * depth, depth), depth)
+        return down_full.at[:, at] if w == 2 else joined.at[pl.ds(w * pitch, slab), at]
 
     def spot(w, j, row=m):
         a, b, c = plane[j]
@@ -509,6 +512,24 @@
     with jax.named_scope("A_flip"):
         loads[0].wait()
         flip_weights(0)
+    with jax.named_scope("A_barrier"):
+        pl.semaphore_wait(barrier, n)
+    loads[10].wait()
+    if pitch > slab:
+        for w in range(2):
+            joined[w * pitch + slab:(w + 1) * pitch, :] = jnp.zeros(
+                (pitch - slab, joined.shape[1]), BF16)
+
+    def send_inner(w, s):
+        @pl.when(inner)
+        def _():
+            send_b(w, s)
+
+    send_x(0, 1)
+    send_z(0, 0)
+    send_y(0, 0)
+    send_inner(0, 0)
+    send_c(0, 0, 1)
     with jax.named_scope("A_param"):
         for copy in loads[2:5]:
             copy.wait()
@@ -546,20 +567,6 @@
                 turn[...], x_raw[:, b * cb:(b + 1) * cb], (((0,), (0,)), ((), ())),
                 preferred_element_type=F32,
             ).astype(BF16)
-    with jax.named_scope("A_barrier"):
-        pl.semaphore_wait(barrier, n)
-    loads[10].wait()
-
-    def send_inner(w, s):
-        @pl.when(inner)
-        def _():
-            send_b(w, s)
-
-    send_x(0, 1)
-    send_z(0, 0)
-    send_y(0, 0)
-    send_inner(0, 0)
-    send_c(0, 0, 1)
     with jax.named_scope("A_flip1"):
         loads[1].wait()
         flip_weights(1)
@@ -616,6 +623,26 @@
                 er, ei = er + sr[chunk:chunk + 1], ei + si[chunk:chunk + 1]
             total[b, :, :sb] = er
             total[b, :, sb:] = ei
+
+    def pass_z(w, s):
+        with jax.named_scope(f"z{w}{s}"):
+            wait_z(w, s)
+
+        @pl.when(inner)
+        def _():
+            relay(w, s)
+
+        send_y(w, 2 + s)
+
+    def pass_e(w, s):
+        with jax.named_scope(f"e{w}{s}"):
+            wait_e(w, s)
+        send_y(w, 4 + s)
+
+    def pass_l(w, s):
+        with jax.named_scope(f"l{w}{s}"):
+            wait_l(w, s)
+        send_y(w, 6 + s)
 
     here = m * 2 + v
     level = h * 2 + u
@@ -674,6 +701,7 @@
     send_c(0, 0, 0)
     for copy in loads[11:]:
         copy.wait()
+    pass_z(0, 0)
     with jax.named_scope("C_states2"):
         for k, (a, b) in enumerate(((h, ou), (oh, u), (oh, ou))):
             arrive(planes.at[a * 2 + b], to_x, ("plane", k))
@@ -682,6 +710,9 @@
     send_c(0, 1, 0)
     send_c(0, 1, 1)
     send_y(0, 1)
+    send_z(1, 0)
+    send_inner(1, 0)
+    send_z(2, 0)
 
     def second(b):
         lr, li = power_of(b, span)
@@ -713,36 +744,8 @@
             turn[...], mixed, preferred_element_type=F32
         ).astype(BF16)
 
-    def pass_z(w, s):
-        with jax.named_scope(f"z{w}{s}"):
-            wait_z(w, s)
-
-        @pl.when(inner)
-        def _():
-            relay(w, s)
-
-        send_y(w, 2 + s)
-
-    def pass_e(w, s):
-        with jax.named_scope(f"e{w}{s}"):
-            wait_e(w, s)
-        send_y(w, 4 + s)
-
-    def pass_l(w, s):
-        with jax.named_scope(f"l{w}{s}"):
-            wait_l(w, s)
-        send_y(w, 6 + s)
-
     with jax.named_scope("D_scan2a"):
         @pl.loop(0, blocks // 2)
-        def _(b):
-            second(b)
-
-    pass_z(0, 0)
-    send_z(1, 0)
-    send_inner(1, 0)
-    with jax.named_scope("D_scan2b"):
-        @pl.loop(blocks // 2, blocks)
         def _(b):
             second(b)
 
@@ -751,9 +754,16 @@
         wait_x(1, 1)
     send_z(1, 1)
     send_inner(1, 1)
+    with jax.named_scope("D_scan2b"):
+        @pl.loop(blocks // 2, blocks)
+        def _(b):
+            second(b)
+
     with jax.named_scope("D_x10"):
         wait_x(1, 0)
     send_y(1, 1)
+    send_c(1, 0, 1)
+    send_c(1, 1, 1)
 
     tile = min(512, width)
     with jax.named_scope("E_outproj"):
@@ -797,20 +807,28 @@
     def wait_core(k):
         arrive(rows_ref.at[1, k], to_t, ("t", k))
 
-    def product(k, w):
+    def product(k, at):
         block = rows_ref[:, k].reshape(2 * keep_rows, width)
-        return lax.dot_general(block, weights[w][...], across, preferred_element_type=F32)
+        return lax.dot_general(block, joined[at, :], across, preferred_element_type=F32)
+
+    def keep_hidden(k, gate, up):
+        result = (jax.nn.silu(gate) * up).astype(BF16)
+        for t in range(2):
+            hidden[pl.ds((4 * t + k) * keep_rows, keep_rows), :] = (
+                result[t * keep_rows:(t + 1) * keep_rows])
 
     def gate_part(k):
         with jax.named_scope(f"gate{k}"):
-            gates[k] = product(k, 0)
+            gates[k] = product(k, pl.ds(0, slab))
 
     def up_part(k):
         with jax.named_scope(f"up{k}"):
-            result = (jax.nn.silu(gates[k]) * product(k, 1)).astype(BF16)
-            for t in range(2):
-                hidden[pl.ds((4 * t + k) * keep_rows, keep_rows), :] = (
-                    result[t * keep_rows:(t + 1) * keep_rows])
+            keep_hidden(k, gates[k], product(k, pl.ds(pitch, slab)))
+
+    def both_parts(k):
+        with jax.named_scope(f"both{k}"):
+            result = product(k, pl.ds(0, 2 * pitch))
+            keep_hidden(k, result[:, :slab], result[:, pitch:pitch + slab])
 
     def first_rows():
         with jax.named_scope("r1"):
@@ -836,7 +854,6 @@
         send_inner(2, 0)
         wait_x(2, 1)
         send_inner(2, 1)
-        send_z(2, 0)
         send_z(2, 1)
         wait_x(2, 0)
         send_y(2, 1)
@@ -857,7 +874,6 @@
             wait_core(k)
 
     for s in range(2):
-        send_c(1, s, 1)
         send_c(1, s, 0)
     pass_e(0, 0)
     pass_e(0, 1)
@@ -887,20 +903,19 @@
     relay_rows(3)
     up_part(1)
     core_rows(2)
-    gate_part(2)
     pass_z(2, 0)
+    both_parts(2)
     last_rows()
-    up_part(2)
+    pass_z(2, 1)
     core_rows(3)
-    gate_part(3)
-    up_part(3)
+    both_parts(3)
     pass_e(2, 0)
     with jax.named_scope("moves"):
         for copy in moves:
             copy.wait_send()
 
     across_u = width // 8
-    chunks = [(h, h, m), (h, oh, m), (oh, h, m), (h, h, om), (h, oh, om), (oh, oh, m),
+    chunks = [(h, h, m), (h, oh, m), (h, h, om), (h, oh, om), (oh, h, m), (oh, oh, m),
               (oh, h, om), (oh, oh, om)]
 
     def columns(j):
@@ -908,16 +923,19 @@
         return pl.ds(pl.multiple_of(index(a, b, c, 0) * depth, across_u), across_u)
 
     def down(j):
-        at = columns(j)
+        pair_of = (2 * j, 2 * j + 1)
+        right = jnp.concatenate([down_full[:, columns(i)] for i in pair_of], axis=1)
         for t in (1, 0):
             result = jnp.dot(
-                hidden[4 * t * keep_rows:4 * (t + 1) * keep_rows, :], weights[2][:, at],
+                hidden[4 * t * keep_rows:4 * (t + 1) * keep_rows, :], right,
                 preferred_element_type=F32,
             ).astype(BF16)
-            for k in range(4):
-                rows_ref[t, k, :, at] = result[k * keep_rows:(k + 1) * keep_rows]
-            if t:
-                send(rows_ref.at[1, :, :, at], partners.at[j], to_t, ("p", j))
+            for side, i in enumerate(pair_of):
+                for k in range(4):
+                    rows_ref[t, k, :, columns(i)] = result[
+                        k * keep_rows:(k + 1) * keep_rows, side * across_u:(side + 1) * across_u]
+                if t:
+                    send(rows_ref.at[1, :, :, columns(i)], partners.at[i], to_t, ("p", i))
 
     def add(target, j, other):
         at = columns(j)
@@ -950,6 +968,8 @@
         arrive(firsts.at[j, 1], device, ("f", j, 1))
         add(0, j, firsts.at[j, 1])
 
+    stored = []
+
     def finish(j):
         at = columns(j)
         arrive(seconds.at[j], to_z if X_FIRST[j] else to_x, ("g", j))
@@ -961,28 +981,13 @@
             summed = summed.astype(BF16).astype(F32)
             out_ref[lines, at] = (carried_ref[lines, at] + 0.5 * summed).astype(BF16)
 
-    order = ("d0", "z", "p0", "d1", "e", "d2", "p1", "d3", "p2", "c0", "d4", "p3", "c1", "l", "d5",
-             "p4", "c2", "f0", "d6", "p5", "c3", "f1", "d7", "p6", "c4", "f2", "p7", "c5", "f3",
-             "c6", "f4", "c7", "f5", "f6", "f7")
-    relayed, passed = next(counter), next(counter)
-    inside.append((("l", 2, 1), relayed))
-    everywhere.append(describe(extra.at[0], extra.at[0], to_y, ("y", 2, 3), passed))
-
-    def late_z(kind):
-        @pl.when(is_inner == kind)
-        def _():
-            wait_z(2, 1)
-            if kind:
-                describe(spot(2, 3), spot(2, 3), to_c, ("l", 2, 1), relayed).start()
-            describe(spot(2, 3), spot(2, 3), to_y, ("y", 2, 3), passed).start()
-
-    with jax.named_scope("z21"):
-        late_z(1)
+        copy = pltpu.make_async_copy(out_ref.at[:, at], out_hbm.at[:, at], out_sem.at[j])
+        copy.start()
+        stored.append(copy)
+
+    order = ORDER
     stages = {"d": down, "p": pair, "c": combine, "f": finish}
     for word in order:
-        if word == "z":
-            late_z(0)
-            continue
         if word == "e":
             pass_e(2, 1)
             continue
@@ -991,19 +996,24 @@
             pass_l(2, 1)
             continue
         j = int(word[1])
-        if word in ("d3", "d6", "d7"):
+        if word in ("d1", "d3"):
             with jax.named_scope("y2" + word):
-                for i in {"d3": (0, 1, 2, 3), "d6": (4, 5), "d7": (6, 7)}[word]:
+                for i in range(4 * (j // 2), 4 * (j // 2) + 4):
                     wait_y(2, i)
         with jax.named_scope({"d": "down", "p": "pair", "c": "comb", "f": "fin"}[word[0]] + word[1]):
             stages[word[0]](j)
-    for copy in everywhere:
-        copy.wait_send()
-
-    @pl.when(inner)
-    def _():
-        for name, number in inside:
-            describe(extra.at[0], extra.at[0], to_c, name, number).wait_send()
+    with jax.named_scope("end_sends"):
+        for copy in everywhere:
+            copy.wait_send()
+
+        @pl.when(inner)
+        def _():
+            for name, number in inside:
+                describe(extra.at[0], extra.at[0], to_c, name, number).wait_send()
+
+    with jax.named_scope("end_store"):
+        for copy in stored:
+            copy.wait()
 
 
 def shift(value, axis, count, by):
@@ -1028,13 +1038,17 @@
     vmem = pl.BlockSpec(memory_space=pltpu.VMEM)
     if depth % 128 == 0 and (tp, nh, nm) == (2, 2, 2):
         cut = width // 8
+        pitch = -(-part // 128) * 128
         return pl.pallas_call(
             functools.partial(streamed, sizes),
             in_specs=[pl.BlockSpec(memory_space=pl.ANY)] * 15,
-            out_specs=vmem,
+            out_specs=pl.BlockSpec(memory_space=pl.ANY),
             out_shape=jax.ShapeDtypeStruct((keep_rows, width), BF16),
             scratch_shapes=[
-                *[pltpu.VMEM((part, n * depth), BF16)] * 3,
+                pltpu.VMEM((keep_rows, width), BF16),
+                pltpu.SemaphoreType.DMA((8,)),
+                pltpu.VMEM((2 * pitch, n * depth), BF16),
+                pltpu.VMEM((part, n * depth), BF16),
                 pltpu.VMEM((3, part, depth), BF16),
                 pltpu.VMEM((2, 4, keep_rows, width), BF16),
                 pltpu.VMEM((keep_rows, width), F32),
@@ -1070,8 +1084,8 @@
                 pltpu.VMEM((hidden_units, depth), BF16),
                 pltpu.VMEM((blocks, 2, sb), F32),
                 pltpu.VMEM((blocks, 2, sb), F32),
-                pltpu.SemaphoreType.DMA((160,)),
-                pltpu.SemaphoreType.DMA((160,)),
+                pltpu.SemaphoreType.DMA((106,)),
+                pltpu.SemaphoreType.DMA((100,)),
                 pltpu.SemaphoreType.DMA((3,)),
                 pltpu.SemaphoreType.DMA((15,)),
             ],

time: 147 us -> 143 us (0.973)
  Pallas kernels: 145 us -> 140 us
    pallas_call x1, Pallas kernels: 145 us -> 140 us  [on_device(): pl.pallas_call(functools.partial(streamed, sizes), in_specs=[pl.BlockSpec...]
where the time goes in v4:
time: 143 us
  Pallas kernels  140 us (98%)
  local copies, waits for them, and re-layouts  2.3 us (2%)
    pallas_call x1, Pallas kernels, on_device(): pl.pallas_call(functools.partial(streamed, sizes), in_specs=[pl.BlockSpec...  140 us

profile of v4, /device:TPU:0, one launch (start us, length us, event | category | flops | bytes accessed | tf_op | source)
XLA Modules:
  0.0 142.8 jit_solution(512211368512137828)
XLA Ops:
  0.0 140.5 %streamed.1 = bf16[256,2048]{1,0:T(8,128)(2,1)} custom-call(bf16[512,512]{1,0:T(8,128)(2,1)} %x_hbm.1, bf16[256,2048]{1,0:T(8,128)(2,1)} %residual_hbm.1, f32[32,64]{1,0:T(8,128)} %decay_re.1, f32[32,64]{1,0:T(8,128)} %decay_im.1, f32[1,32]{1,0:T(1,128)} %bitcast.17, f32[512,64]{1,0:T(8,128)} %bitcast.11, f32[512,64]{1,0:T(8,128)} %bitcast.12, ...), custom_call_target="tpu_custom_call" | custom-call | tf_op jit(solution)/shard_map/streamed/pallas_call | solution.py:1042
  140.5 2.3 %copy.17 = bf16[256,2048]{1,0:T(8,128)(2,1)} copy(bf16[256,2048]{1,0:T(8,128)(2,1)} %streamed.1) | data formatting | bytes 2097152

commit v5 on v4

--- a/solution.py
+++ b/solution.py
@@ -402,7 +402,8 @@
     is_inner = lax.rem(h + u, 2)
     inner = is_inner == 1
     across = (((1,), (1,)), ((), ()))
-    slots, everywhere, inside, moves = {}, [], [], []
+    slots, everywhere, moves = {}, [], []
+    groups_of, fixed = {}, {}
     counter = iter(range(send_sem.shape[0]))
 
     def slot(name):
@@ -414,11 +415,18 @@
             recv_sem=recv_sem.at[slot(name) if isinstance(name, tuple) else name], device_id=device, device_id_type=MESH,
         )
 
-    def send(src, dst, device, name, kept=everywhere):
-        number = next(counter)
+    def group_number(group):
+        if group not in fixed:
+            fixed[group] = next(counter)
+        groups_of[group] = groups_of.get(group, 0) + 1
+        return fixed[group]
+
+    def send(src, dst, device, name, kept=everywhere, group=None):
+        number = next(counter) if group is None else group_number(group)
         copy = describe(src, dst, device, name, number)
         copy.start()
-        kept.append((name, number) if kept is inside else copy)
+        if group is None:
+            kept.append(copy)
 
     def arrive(dst, device, name):
         describe(dst, dst, device, name, 0).wait_recv()
@@ -440,20 +448,19 @@
 
     def send_x(w, s):
         if s:
-            send(mine(w, ou, ov), extra.at[w], to_x, ("xo", w))
+            send(mine(w, ou, ov), extra.at[w], to_x, ("xo", w), group=("w", w))
         else:
-            send(mine(w, u, ov), spot(w, 0), to_x, ("xu", w))
+            send(mine(w, u, ov), spot(w, 0), to_x, ("xu", w), group=("w", w))
 
     def send_z(w, s):
-        send(extra.at[w] if s else mine(w, ou, v), spot(w, s), to_z, ("z", w, s))
+        send(extra.at[w] if s else mine(w, ou, v), spot(w, s), to_z, ("z", w, s), group=("w", w))
 
     numbers = {}
 
     def send_c(w, s, kind):
-        number = numbers.setdefault((w, s), None) or next(counter)
-        if numbers[w, s] is None:
-            numbers[w, s] = number
-            everywhere.append(describe(extra.at[0], extra.at[0], to_c, ("e", w, s), number))
+        if (w, s) not in numbers:
+            numbers[w, s] = group_number(("w", w))
+        number = numbers[w, s]
         name = ("e" if kind else "l", w, s)
 
         @pl.when(is_inner == kind)
@@ -461,13 +468,13 @@
             describe(spot(w, 1) if s else own(w), spot(w, s), to_c, name, number).start()
 
     def send_b(w, s):
-        send(extra.at[w] if s else mine(w, ou, v), spot(w, s), to_b, ("e", w, s), inside)
+        send(extra.at[w] if s else mine(w, ou, v), spot(w, s), to_b, ("e", w, s), group="inside")
 
     def relay(w, s):
-        send(spot(w, 2 + s), spot(w, 2 + s), to_c, ("l", w, s), inside)
+        send(spot(w, 2 + s), spot(w, 2 + s), to_c, ("l", w, s), group="inside")
 
     def send_y(w, j):
-        send(own(w) if j == 0 else spot(w, j), spot(w, j), to_y, ("y", w, j))
+        send(own(w) if j == 0 else spot(w, j), spot(w, j), to_y, ("y", w, j), group=("w", w))
 
     def wait_x(w, s):
         if s:
@@ -712,7 +719,6 @@
     send_y(0, 1)
     send_z(1, 0)
     send_inner(1, 0)
-    send_z(2, 0)
 
     def second(b):
         lr, li = power_of(b, span)
@@ -854,6 +860,7 @@
         send_inner(2, 0)
         wait_x(2, 1)
         send_inner(2, 1)
+        send_z(2, 0)
         send_z(2, 1)
         wait_x(2, 0)
         send_y(2, 1)
@@ -935,7 +942,7 @@
                     rows_ref[t, k, :, columns(i)] = result[
                         k * keep_rows:(k + 1) * keep_rows, side * across_u:(side + 1) * across_u]
                 if t:
-                    send(rows_ref.at[1, :, :, columns(i)], partners.at[i], to_t, ("p", i))
+                    send(rows_ref.at[1, :, :, columns(i)], partners.at[i], to_t, ("p", i), group="p")
 
     def add(target, j, other):
         at = columns(j)
@@ -954,7 +961,7 @@
         arrive(partners.at[j], to_t, ("p", j))
         for place_in, k in enumerate((3, near)):
             add(k, j, partners.at[j, k])
-            send(rows_ref.at[0, k, :, at], firsts.at[j, place_in], device, ("f", j, place_in))
+            send(rows_ref.at[0, k, :, at], firsts.at[j, place_in], device, ("f", j, place_in), group="f")
         add(far, j, partners.at[j, far])
         add(0, j, partners.at[j, 0])
 
@@ -964,7 +971,7 @@
         device, other = (to_x, to_z) if X_FIRST[j] else (to_z, to_x)
         arrive(firsts.at[j, 0], device, ("f", j, 0))
         add(far, j, firsts.at[j, 0])
-        send(rows_ref.at[0, far, :, at], seconds.at[j], other, ("g", j))
+        send(rows_ref.at[0, far, :, at], seconds.at[j], other, ("g", j), group="g")
         arrive(firsts.at[j, 1], device, ("f", j, 1))
         add(0, j, firsts.at[j, 1])
 
@@ -1002,14 +1009,21 @@
                     wait_y(2, i)
         with jax.named_scope({"d": "down", "p": "pair", "c": "comb", "f": "fin"}[word[0]] + word[1]):
             stages[word[0]](j)
+    def drain(group, ref):
+        describe(ref, ref, to_x, ("mix",), fixed[group]).wait_send()
+
     with jax.named_scope("end_sends"):
         for copy in everywhere:
             copy.wait_send()
+        for w in range(3):
+            drain(("w", w), down_full.at[:, pl.ds(0, groups_of["w", w] * depth)])
+        drain("p", partners)
+        drain("f", firsts)
+        drain("g", seconds)
 
         @pl.when(inner)
         def _():
-            for name, number in inside:
-                describe(extra.at[0], extra.at[0], to_c, name, number).wait_send()
+            drain("inside", down_full.at[:, pl.ds(0, groups_of["inside"] * depth)])
 
     with jax.named_scope("end_store"):
         for copy in stored:
@@ -1084,7 +1098,7 @@
                 pltpu.VMEM((hidden_units, depth), BF16),
                 pltpu.VMEM((blocks, 2, sb), F32),
                 pltpu.VMEM((blocks, 2, sb), F32),
-                pltpu.SemaphoreType.DMA((106,)),
+                pltpu.SemaphoreType.DMA((27,)),
                 pltpu.SemaphoreType.DMA((100,)),
                 pltpu.SemaphoreType.DMA((3,)),
                 pltpu.SemaphoreType.DMA((15,)),

time: 143 us -> 141 us (0.986)
    pallas_call x1, Pallas kernels: 140 us -> 139 us  [on_device(): pl.pallas_call(functools.partial(streamed, sizes), in_specs=[pl.BlockSpec...]
where the time goes in v5:
time: 141 us
  Pallas kernels  139 us (99%)
  local copies, waits for them, and re-layouts  2.3 us (2%)
    pallas_call x1, Pallas kernels, on_device(): pl.pallas_call(functools.partial(streamed, sizes), in_specs=[pl.BlockSpec...  139 us

profile of v5, /device:TPU:0, one launch (start us, length us, event | category | flops | bytes accessed | tf_op | source)
XLA Modules:
  0.0 140.9 jit_solution(3968316832676490741)
XLA Ops:
  0.0 138.6 %streamed.1 = bf16[256,2048]{1,0:T(8,128)(2,1)} custom-call(bf16[512,512]{1,0:T(8,128)(2,1)} %x_hbm.1, bf16[256,2048]{1,0:T(8,128)(2,1)} %residual_hbm.1, f32[32,64]{1,0:T(8,128)} %decay_re.1, f32[32,64]{1,0:T(8,128)} %decay_im.1, f32[1,32]{1,0:T(1,128)} %bitcast.17, f32[512,64]{1,0:T(8,128)} %bitcast.11, f32[512,64]{1,0:T(8,128)} %bitcast.12, ...), custom_call_target="tpu_custom_call" | custom-call | tf_op jit(solution)/shard_map/streamed/pallas_call | solution.py:1056
  138.6 2.3 %copy.17 = bf16[256,2048]{1,0:T(8,128)(2,1)} copy(bf16[256,2048]{1,0:T(8,128)(2,1)} %streamed.1) | data formatting | bytes 2097152

commit v6 on v5

--- a/solution.py
+++ b/solution.py
@@ -16,8 +16,8 @@
 CHUNKS = 8
 X_FIRST = (1, 1, 1, 0, 1, 0, 1, 0)
 PIECES = 4
-ORDER = ("d0", "e", "p0", "p1", "d1", "p2", "p3", "l", "d2", "p4", "p5", "c0", "d3", "p6", "p7",
-         "c1", "c2", "c3", "c4", "c5", "f0", "f1", "c6", "c7", "f2", "f3", "f4", "f5", "f6", "f7")
+ORDER = ("d0", "e", "p0", "p1", "d1", "p2", "p3", "l", "d2", "p4", "p5", "c0", "c1", "d3", "p6",
+         "p7", "c2", "c3", "c4", "c5", "f0", "f1", "c6", "c7", "f2", "f3", "f4", "f5", "f6", "f7")
 MESH = pl.DeviceIdType.MESH
 
 
@@ -474,7 +474,7 @@
         send(spot(w, 2 + s), spot(w, 2 + s), to_c, ("l", w, s), group="inside")
 
     def send_y(w, j):
-        send(own(w) if j == 0 else spot(w, j), spot(w, j), to_y, ("y", w, j), group=("w", w))
+        send(own(w) if j == 0 else spot(w, j), spot(w, j), to_y, yname(w, j), group=("w", w))
 
     def wait_x(w, s):
         if s:
@@ -491,8 +491,14 @@
     def wait_l(w, s):
         arrive(spot(w, 6 + s), to_c, ("l", w, s))
 
-    def wait_y(w, j):
-        arrive(spot(w, j, om), to_y, ("y", w, j))
+    def yname(w, j):
+        return ("y", w, j // 4 if w == 2 else 0)
+
+    def wait_y(w, part):
+        count = 4 if w == 2 else 8
+        at = pl.ds(0, count * depth)
+        ref = down_full.at[:, at] if w == 2 else joined.at[pl.ds(w * pitch, slab), at]
+        arrive(ref, to_y, ("y", w, part))
 
     barrier = pltpu.get_barrier_semaphore()
     others_sp = []
@@ -873,8 +879,7 @@
 
     def whole(w):
         with jax.named_scope(f"y{w}"):
-            for j in range(8):
-                wait_y(w, j)
+            wait_y(w, 0)
 
     def core_rows(k):
         with jax.named_scope(f"t{k}"):
@@ -1005,8 +1010,7 @@
         j = int(word[1])
         if word in ("d1", "d3"):
             with jax.named_scope("y2" + word):
-                for i in range(4 * (j // 2), 4 * (j // 2) + 4):
-                    wait_y(2, i)
+                wait_y(2, j // 2)
         with jax.named_scope({"d": "down", "p": "pair", "c": "comb", "f": "fin"}[word[0]] + word[1]):
             stages[word[0]](j)
     def drain(group, ref):
@@ -1099,7 +1103,7 @@
                 pltpu.VMEM((blocks, 2, sb), F32),
                 pltpu.VMEM((blocks, 2, sb), F32),
                 pltpu.SemaphoreType.DMA((27,)),
-                pltpu.SemaphoreType.DMA((100,)),
+                pltpu.SemaphoreType.DMA((80,)),
                 pltpu.SemaphoreType.DMA((3,)),
                 pltpu.SemaphoreType.DMA((15,)),
             ],

time: 141 us -> 141 us (level)
  no operation moved by 1% of the time
where the time goes in v6:
time: 141 us
  Pallas kernels  138 us (98%)
  local copies, waits for them, and re-layouts  2.3 us (2%)
    pallas_call x1, Pallas kernels, on_device(): pl.pallas_call(functools.partial(streamed, sizes), in_specs=[pl.BlockSpec...  138 us

profile of v6, /device:TPU:0, one launch (start us, length us, event | category | flops | bytes accessed | tf_op | source)
XLA Modules:
  0.0 140.7 jit_solution(10169689117240953571)
XLA Ops:
  0.0 138.4 %streamed.1 = bf16[256,2048]{1,0:T(8,128)(2,1)} custom-call(bf16[512,512]{1,0:T(8,128)(2,1)} %x_hbm.1, bf16[256,2048]{1,0:T(8,128)(2,1)} %residual_hbm.1, f32[32,64]{1,0:T(8,128)} %decay_re.1, f32[32,64]{1,0:T(8,128)} %decay_im.1, f32[1,32]{1,0:T(1,128)} %bitcast.17, f32[512,64]{1,0:T(8,128)} %bitcast.11, f32[512,64]{1,0:T(8,128)} %bitcast.12, ...), custom_call_target="tpu_custom_call" | custom-call | tf_op jit(solution)/shard_map/streamed/pallas_call | solution.py:1060
  138.4 2.3 %copy.17 = bf16[256,2048]{1,0:T(8,128)(2,1)} copy(bf16[256,2048]{1,0:T(8,128)(2,1)} %streamed.1) | data formatting | bytes 2097152
